TPU v7x, 32 devices: a whole 2x2x4 slice. The times are simulated.
32 devices in a mesh: sp: 16 (over z, y, x), tp: 2 (over core).
Axes of the slice: x: 2, y: 2, z: 4, core: 2. Of those that a mesh axis runs over, the one named last changes fastest.
Arguments:
- conv_value: bfloat16 [4096, 1024], P('sp', 'tp'), may hold values from -6 to 6
- conv_gate: bfloat16 [4096, 1024], P('sp', 'tp'), may hold values from -6 to 6
- taps: bfloat16 [31, 1024], P(None, 'tp'), may hold values from -1 to 1
- doc_ids: int32 [4096], P('sp'), may hold values from 0 to 3, never falling along the last dimension, each value on 1 to 2048 neighbouring positions
- gn_gain: float32 [1024], P('tp'), may hold values from 0.1 to 1.9
- gn_shift: float32 [1024], P('tp'), may hold values from -3 to 3
- conv_out: bfloat16 [1024, 2048], replicated, may hold values from -0.1875 to 0.1875
- residual: bfloat16 [4096, 2048], P(('sp', 'tp')), may hold values from -6 to 6
- norm_gain: float32 [2048], replicated, may hold values from 0.1 to 1.9
- routes: int32 [4096, 2], P(('sp', 'tp')), may hold values from 0 to 31, as said below
- route_weight: float32 [4096, 2], P(('sp', 'tp')), may hold values from 0.3 to 1.2
- expert_gate: bfloat16 [32, 2048, 512], P(('sp', 'tp')), may hold values from -0.125 to 0.125
- expert_up: bfloat16 [32, 2048, 512], P(('sp', 'tp')), may hold values from -0.125 to 0.125
- expert_down: bfloat16 [32, 512, 2048], P(('sp', 'tp')), may hold values from -0.25 to 0.25
- shared_gate: bfloat16 [2048, 512], replicated, may hold values from -0.125 to 0.125
- shared_up: bfloat16 [2048, 512], replicated, may hold values from -0.125 to 0.125
- shared_down: bfloat16 [512, 2048], replicated, may hold values from -0.25 to 0.25
Outputs:
- layer_out: bfloat16 [4096, 2048], P(('sp', 'tp'))
Inputs may be any that keep to these rules, and one draw needn't show every extreme that they name: `routes`: each row names 2 different experts. The rows of one device name each expert at most 16 times, and one expert, the same for every device, exactly 16 times. `doc_ids`: numbers never fall from one position to the next.
All inputs are finite; a program needn't handle non-finite values.
Results may differ from a plain program's by a relative error of at most 0.014.
Values may be sent and summed in bfloat16 or wider, within the bound.
A program may use at most 128 MiB of HBM per device.

v0:
```python
import functools

import jax
import jax.numpy as jnp
from jax import lax
from jax.experimental import pallas as pl
from jax.experimental.pallas import tpu as pltpu
from jax.sharding import PartitionSpec as P

GROUPS = 8


epsilon = 1e-06


def from_behind(x, axis, by):
    peers = lax.axis_size(axis)
    pairs = [(i, i + by) for i in range(peers) if 0 <= i + by < peers]
    return lax.ppermute(x, axis, pairs)


def per_device(
    conv_value,
    conv_gate,
    taps,
    doc_ids,
    gn_gain,
    gn_shift,
    conv_out,
    residual,
    norm_gain,
    routes,
    route_weight,
    expert_gate,
    expert_up,
    expert_down,
    shared_gate,
    shared_up,
    shared_down,
):
    position_count, channel_count = conv_value.shape
    kernel_width = taps.shape[0]
    model_width = residual.shape[1]
    glu_out = (
        conv_value.astype(jnp.float32) * jax.nn.sigmoid(conv_gate.astype(jnp.float32))
    ).astype(jnp.bfloat16)
    rim_start = position_count - kernel_width + 1
    edge_glu, edge_ids = from_behind((glu_out[rim_start:], doc_ids[rim_start:]), "sp", 1)
    longer_glu = jnp.concatenate([edge_glu, glu_out], axis=0)
    longer_ids = jnp.concatenate([edge_ids, doc_ids], axis=0)
    conv_sum = jnp.zeros((position_count, channel_count), jnp.float32)
    for offset in range(kernel_width):
        same_doc = (longer_ids[offset : offset + position_count] == doc_ids)[:, None]
        tap_term = taps[offset].astype(jnp.float32)[None, :] * longer_glu[
            offset : offset + position_count
        ].astype(jnp.float32)
        conv_sum = conv_sum + jnp.where(same_doc, tap_term, 0.0)
    core_split = lax.axis_size("tp")
    groups_here = GROUPS // core_split
    grouped = conv_sum.reshape(position_count, groups_here, channel_count // groups_here)
    group_mean = jnp.mean(grouped, axis=-1, keepdims=True)
    centered = grouped - group_mean
    group_var = jnp.mean(centered * centered, axis=-1, keepdims=True)
    normalized = (centered * lax.rsqrt(group_var + epsilon)).reshape(position_count, channel_count)
    conv_act = jax.nn.silu(normalized * gn_gain + gn_shift).astype(jnp.bfloat16)
    token_rows = lax.all_to_all(conv_act, "tp", split_axis=0, concat_axis=1, tiled=True)
    projected = jnp.dot(token_rows, conv_out, preferred_element_type=jnp.float32)
    stream = (residual.astype(jnp.float32) + projected).astype(jnp.bfloat16)
    stream_wide = stream.astype(jnp.float32)
    normed = (
        stream_wide
        * lax.rsqrt(jnp.mean(stream_wide * stream_wide, axis=-1, keepdims=True) + epsilon)
        * norm_gain
    ).astype(jnp.bfloat16)
    token_count, top_count = routes.shape
    sequence_split = lax.axis_size("sp")
    device_count = sequence_split * core_split
    local_experts = expert_gate.shape[0]
    experts = local_experts * device_count
    capacity = 2 * token_count * top_count // experts
    flat_routes = routes.reshape(-1)
    onehot = (flat_routes[:, None] == jnp.arange(experts, dtype=jnp.int32)[None, :]).astype(
        jnp.int32
    )
    slot_index = jnp.sum(jnp.cumsum(onehot, axis=0) * onehot, axis=1) - 1
    target = flat_routes * capacity + slot_index
    source = (
        jnp.full((experts * capacity,), token_count, jnp.int32)
        .at[target]
        .set(jnp.arange(token_count * top_count, dtype=jnp.int32) // top_count)
    )
    padded_rows = jnp.concatenate([normed, jnp.zeros((1, model_width), normed.dtype)], axis=0)
    outgoing = padded_rows[source]
    shared_hidden = (
        jax.nn.silu(jnp.dot(normed, shared_gate, preferred_element_type=jnp.float32))
        * jnp.dot(normed, shared_up, preferred_element_type=jnp.float32)
    ).astype(jnp.bfloat16)
    shared_out = jnp.dot(shared_hidden, shared_down, preferred_element_type=jnp.float32)
    parcel = outgoing.reshape(device_count, local_experts, capacity, model_width)
    arrived = lax.all_to_all(parcel, ("sp", "tp"), split_axis=0, concat_axis=0, tiled=True)
    expert_rows = arrived[:, 0].reshape(-1, model_width)
    gate_part = jnp.dot(expert_rows, expert_gate[0], preferred_element_type=jnp.float32)
    up_part = jnp.dot(expert_rows, expert_up[0], preferred_element_type=jnp.float32)
    hidden = (jax.nn.silu(gate_part) * up_part).astype(jnp.bfloat16)
    result = jnp.dot(hidden, expert_down[0], preferred_element_type=jnp.float32).astype(
        jnp.bfloat16
    )
    results = [result.reshape(arrived.shape[0], arrived.shape[2], model_width)]
    returned = lax.all_to_all(
        jnp.stack(results, axis=1), ("sp", "tp"), split_axis=0, concat_axis=0, tiled=True
    )
    picked = returned.reshape(experts * capacity, model_width)[target].reshape(
        token_count, top_count, model_width
    )
    routed = jnp.zeros((token_count, model_width), jnp.float32)
    for route_index in range(top_count):
        routed = routed + route_weight[:, route_index, None] * picked[:, route_index].astype(
            jnp.float32
        )
    return (stream_wide + shared_out + routed).astype(jnp.bfloat16)


F32 = jnp.float32
BF16 = jnp.bfloat16
MESH_ID = pl.DeviceIdType.MESH
HALO = 32
CHUNK = 32


def flip(index, bits):
    out, weight = index, 1
    while weight <= bits:
        if (bits // weight) % 2:
            out = out + weight * (1 - 2 * ((index // weight) % 2))
        weight *= 2
    return out


def silu(v):
    return v / (1.0 + jnp.exp(-v))


def fused_kernel(
    n_sp,
    n_tp,
    capacity,
    value_ref,
    gate_ref,
    taps_ref,
    ids_ref,
    gain_ref,
    shift_ref,
    resid_ref,
    ngain_ref,
    routes_ref,
    weight_ref,
    conv_out_hbm,
    eg_hbm,
    eu_hbm,
    ed_hbm,
    sg_hbm,
    su_hbm,
    sd_hbm,
    out_ref,
    glu_ext,
    ids_ext,
    tap_rows,
    halo_send,
    halo_recv,
    act,
    act_recv,
    normed_ref,
    base_ref,
    far_tokens,
    far_routes,
    far_weight,
    ids_here,
    send_own,
    send_far,
    arrived,
    result,
    returned,
    relayed,
    part_send,
    part_recv,
    conv_out,
    eg,
    eu,
    ed,
    sg,
    su,
    sd,
    w_sem,
    halo_sem,
    act_sem,
    out_send,
    out_recv,
    back_send,
    back_recv,
    far_sem,
):
    n = n_sp * n_tp
    sp, tp = lax.axis_index("sp"), lax.axis_index("tp")
    me = sp * n_tp + tp
    rows, channels = value_ref.shape
    tokens, model = resid_ref.shape
    width = taps_ref.shape[0]
    group = glu_ext.shape[2]
    groups = channels // group

    near = n // 2
    far = flip(me, near)

    def place(index):
        return (index // n_tp, index % n_tp)

    loads = [
        pltpu.make_async_copy(a, b, w_sem.at[i])
        for i, (a, b) in enumerate(
            [
                (conv_out_hbm, conv_out),
                (sg_hbm, sg),
                (su_hbm, su),
                (sd_hbm, sd),
                (eg_hbm, eg),
                (eu_hbm, eu),
                (ed_hbm, ed),
            ]
        )
    ]
    for load in loads:
        load.start()

    barrier = pltpu.get_barrier_semaphore()
    for j in range(1, n):
        pl.semaphore_signal(barrier, inc=1, device_id=place(flip(me, j)), device_id_type=MESH_ID)

    glu = (value_ref[...].astype(F32) * jax.nn.sigmoid(gate_ref[...].astype(F32))).astype(BF16)
    halo_send[...] = glu[rows - HALO :, :]
    for g in range(groups):
        glu_ext[g, pl.ds(HALO, rows), :] = glu[:, g * group : (g + 1) * group].astype(F32)
    for at in range(0, rows, group):
        row = ids_ref[:, at : at + group].astype(F32)
        column = jnp.broadcast_to(row, (group, group)).T
        ids_here[pl.ds(at, group), :] = column
        ids_ext[pl.ds(HALO + at, group), :] = column
    tap_rows[pl.ds(0, width), :] = taps_ref[...].astype(F32)

    pl.semaphore_wait(barrier, n - 1)

    halo_copies = [
        pltpu.make_async_remote_copy(
            src_ref=halo_send,
            dst_ref=halo_recv,
            send_sem=halo_sem.at[0],
            recv_sem=halo_sem.at[1],
            device_id=(sp + 1, tp),
            device_id_type=MESH_ID,
        ),
        pltpu.make_async_remote_copy(
            src_ref=ids_here.at[pl.ds(rows - HALO, HALO)],
            dst_ref=ids_ext.at[pl.ds(0, HALO)],
            send_sem=halo_sem.at[2],
            recv_sem=halo_sem.at[3],
            device_id=(sp + 1, tp),
            device_id_type=MESH_ID,
        ),
    ]

    @pl.when(sp < n_sp - 1)
    def _():
        for copy in halo_copies:
            copy.start()

    @pl.when(sp == 0)
    def _():
        glu_ext[:, pl.ds(0, HALO), :] = jnp.zeros((groups, HALO, group), F32)
        ids_ext[pl.ds(0, HALO), :] = jnp.full((HALO, group), -1.0, F32)

    def to_far(src, dst, index):
        return pltpu.make_async_remote_copy(
            src_ref=src,
            dst_ref=dst,
            send_sem=far_sem.at[2 * index],
            recv_sem=far_sem.at[2 * index + 1],
            device_id=place(far),
            device_id_type=MESH_ID,
        )

    routes_copy = to_far(routes_ref, far_routes, 0)
    weight_copy = to_far(weight_ref, far_weight, 1)
    routes_copy.start()
    weight_copy.start()

    slots = near * capacity
    first = (me // near) * near
    tri_r = lax.broadcasted_iota(jnp.int32, (tokens, tokens), 0)
    tri_c = lax.broadcasted_iota(jnp.int32, (tokens, tokens), 1)
    later = (tri_r < tri_c).astype(F32).astype(BF16)
    spread_t = (
        (
            lax.broadcasted_iota(jnp.int32, (slots, near), 0) // capacity
            == lax.broadcasted_iota(jnp.int32, (slots, near), 1)
        )
        .astype(F32)
        .astype(BF16)
    )
    row_slot = (lax.broadcasted_iota(jnp.int32, (slots, tokens), 0) % capacity).astype(F32)
    row_expert = first + lax.broadcasted_iota(jnp.int32, (slots, tokens), 0) // capacity
    expert_row = first + lax.broadcasted_iota(jnp.int32, (near, tokens), 0)

    def tables(routes, weight):
        member = (
            (routes[0:1, :] == expert_row).astype(F32)
            + (routes[1:2, :] == expert_row).astype(F32)
        ).astype(BF16)
        slot = jnp.dot(member, later, preferred_element_type=F32).astype(BF16)
        right = jnp.dot(spread_t, slot, preferred_element_type=F32) == row_slot
        hit0 = jnp.where(right & (routes[0:1, :] == row_expert), 1.0, 0.0)
        hit1 = jnp.where(right & (routes[1:2, :] == row_expert), 1.0, 0.0)
        pick = (hit0 + hit1).astype(BF16)
        mix = (hit0 * weight[0:1, :] + hit1 * weight[1:2, :]).T
        high = mix.astype(BF16)
        return pick, high, (mix - high.astype(F32)).astype(BF16)

    pick, w_high, w_low = tables(routes_ref[...], weight_ref[...])

    @pl.when(sp > 0)
    def _():
        for copy in halo_copies:
            copy.wait_recv()
        for g in range(groups):
            glu_ext[g, pl.ds(0, HALO), :] = halo_recv[:, g * group : (g + 1) * group].astype(F32)

    @pl.when(sp < n_sp - 1)
    def _():
        for copy in halo_copies:
            copy.wait_send()

    def conv_block(start):
        def body(i, carry):
            r = pl.multiple_of(start + i * CHUNK, CHUNK)
            mine = ids_here[pl.ds(r, CHUNK), :]
            sums = [jnp.zeros((CHUNK, group), F32) for _ in range(groups)]
            for tap in range(width):
                off = HALO - width + 1 + tap
                same = ids_ext[pl.ds(r + off, CHUNK), :] == mine
                for g in range(groups):
                    term = (
                        tap_rows[tap : tap + 1, g * group : (g + 1) * group]
                        * glu_ext[g, pl.ds(r + off, CHUNK), :]
                    )
                    sums[g] = sums[g] + jnp.where(same, term, 0.0)
            for g in range(groups):
                cols = slice(g * group, (g + 1) * group)
                centered = sums[g] - jnp.mean(sums[g], axis=-1, keepdims=True)
                var = jnp.mean(centered * centered, axis=-1, keepdims=True)
                v = centered * lax.rsqrt(var + epsilon) * gain_ref[:, cols] + shift_ref[:, cols]
                act[pl.ds(r, CHUNK), cols] = silu(v).astype(BF16)
            return carry

        lax.fori_loop(0, tokens // CHUNK, body, 0)

    other = (tp + 1) % n_tp
    theirs = pl.multiple_of(other * tokens, tokens)
    mine_at = pl.multiple_of(tp * tokens, tokens)
    conv_block(theirs)
    act_copy = pltpu.make_async_remote_copy(
        src_ref=act.at[pl.ds(theirs, tokens)],
        dst_ref=act_recv,
        send_sem=act_sem.at[0],
        recv_sem=act_sem.at[1],
        device_id=(sp, other),
        device_id_type=MESH_ID,
    )
    act_copy.start()
    conv_block(mine_at)
    loads[0].wait()
    half = channels
    projected = jnp.dot(
        act[pl.ds(mine_at, tokens), :],
        conv_out[pl.ds(pl.multiple_of(tp * half, half), half), :],
        preferred_element_type=F32,
    )
    act_copy.wait()
    projected = projected + jnp.dot(
        act_recv[...],
        conv_out[pl.ds(pl.multiple_of(other * half, half), half), :],
        preferred_element_type=F32,
    )
    stream = (resid_ref[...].astype(F32) + projected).astype(BF16).astype(F32)
    base_ref[...] = stream
    normed = (
        stream
        * lax.rsqrt(jnp.mean(stream * stream, axis=-1, keepdims=True) + epsilon)
        * ngain_ref[...]
    ).astype(BF16)
    normed_ref[...] = normed

    per = near // 2
    block = per * capacity

    def piece(index):
        return pl.ds(pl.multiple_of(index * capacity, capacity), capacity)

    def exchange(src, dst, sems, index, peer):
        return pltpu.make_async_remote_copy(
            src_ref=src,
            dst_ref=dst,
            send_sem=sems[0].at[index],
            recv_sem=sems[1].at[index],
            device_id=place(peer),
            device_id_type=MESH_ID,
        )

    out_sems, back_sems = (out_send, out_recv), (back_send, back_recv)
    here = me % near

    def own_out(k):
        peer = flip(me, k)
        return exchange(send_own.at[piece(peer % near)], arrived.at[piece(me)], out_sems, k, peer)

    wide = model // 2

    def far_out(k, part):
        peer = flip(me, k)
        cols = pl.ds(part * wide, wide)
        return exchange(
            send_far.at[piece(peer % near), cols],
            arrived.at[piece(far), cols],
            out_sems,
            near * (part + 1) + k,
            peer,
        )

    def own_back(k):
        peer = flip(me, k)
        return exchange(result.at[piece(peer)], returned.at[piece(here)], back_sems, k, peer)

    def far_back(k):
        peer, source = flip(me, k), flip(me, near + k)
        return exchange(
            result.at[piece(source)], relayed.at[piece(here)], back_sems, near + k, peer
        )

    token_copies = [
        to_far(normed_ref.at[:, pl.ds(p * wide, wide)], far_tokens.at[:, pl.ds(p * wide, wide)], i)
        for p, i in ((0, 2), (1, 4))
    ]
    for copy in token_copies:
        copy.start()
    send_own[...] = jnp.dot(pick, normed_ref[...], preferred_element_type=F32).astype(BF16)
    for k in range(near - 1, 0, -1):
        own_out(k).start()
    arrived[piece(me), :] = send_own[piece(here), :]
    routes_copy.wait()
    weight_copy.wait()
    far_pick, far_high, far_low = tables(far_routes[...], far_weight[...])

    for load in loads[1:4]:
        load.wait()
    shared = (
        silu(jnp.dot(normed_ref[...], sg[...], preferred_element_type=F32))
        * jnp.dot(normed_ref[...], su[...], preferred_element_type=F32)
    ).astype(BF16)
    base_ref[...] += jnp.dot(shared, sd[...], preferred_element_type=F32)
    for load in loads[4:]:
        load.wait()

    def experts(b):
        for low in range(per):
            j = b * per + low
            if j % near:
                if j < near:
                    own_out(j).wait_recv()
                else:
                    far_out(j - near, 0).wait_recv()
                    far_out(j - near, 1).wait_recv()
        at = pl.ds(pl.multiple_of(flip(me // per, b) * block, block), block)
        x = arrived[at, :]
        hidden = (
            silu(jnp.dot(x, eg[0], preferred_element_type=F32))
            * jnp.dot(x, eu[0], preferred_element_type=F32)
        ).astype(BF16)
        result[at, :] = jnp.dot(hidden, ed[0], preferred_element_type=F32).astype(BF16)

    for part in range(2):
        token_copies[part].wait_recv()
        cols = slice(part * wide, (part + 1) * wide)
        send_far[:, cols] = jnp.dot(
            far_pick, far_tokens[:, cols], preferred_element_type=F32
        ).astype(BF16)
        for k in range(near - 1, 0, -1):
            far_out(k, part).start()
    arrived[piece(far), :] = send_far[piece(here), :]

    experts(0)
    for k in range(per - 1, 0, -1):
        own_back(k).start()
    returned[piece(here), :] = result[piece(me), :]
    experts(1)
    experts(2)
    for k in range(per - 1, 0, -1):
        far_back(k).start()
    relayed[piece(here), :] = result[piece(far), :]
    experts(3)
    for k in range(near - 1, per - 1, -1):
        far_back(k).start()

    for k in range(1, near):
        far_back(k).wait_recv()
    back = relayed[...]
    part_send[...] = (
        jnp.dot(far_high, back, preferred_element_type=F32)
        + jnp.dot(far_low, back, preferred_element_type=F32)
    ).astype(BF16)
    part_copy = to_far(part_send, part_recv, 3)
    part_copy.start()
    for k in range(near - 1, per - 1, -1):
        own_back(k).start()

    for k in range(1, near):
        own_back(k).wait_recv()
    back = returned[...]
    base_ref[...] += jnp.dot(w_high, back, preferred_element_type=F32) + jnp.dot(
        w_low, back, preferred_element_type=F32
    )
    part_copy.wait_recv()
    out_ref[...] = (base_ref[...] + part_recv[...].astype(F32)).astype(BF16)
    for k in range(1, near):
        own_out(k).wait_send()
        far_out(k, 0).wait_send()
        far_out(k, 1).wait_send()
        own_back(k).wait_send()
        far_back(k).wait_send()
    for copy in token_copies:
        copy.wait_send()
    part_copy.wait_send()


def fused(
    conv_value,
    conv_gate,
    taps,
    doc_ids,
    gn_gain,
    gn_shift,
    conv_out,
    residual,
    norm_gain,
    routes,
    route_weight,
    expert_gate,
    expert_up,
    expert_down,
    shared_gate,
    shared_up,
    shared_down,
):
    n_sp, n_tp = lax.axis_size("sp"), lax.axis_size("tp")
    n = n_sp * n_tp
    rows, channels = conv_value.shape
    tokens, model = residual.shape
    capacity = 2 * tokens * routes.shape[1] // n
    group = channels * n_tp // GROUPS
    near_slots = n // 2 * capacity
    vmem = pl.BlockSpec(memory_space=pltpu.VMEM)
    hbm = pl.BlockSpec(memory_space=pl.ANY)
    dma = pltpu.SemaphoreType.DMA
    return pl.pallas_call(
        functools.partial(fused_kernel, n_sp, n_tp, capacity),
        out_shape=jax.ShapeDtypeStruct((tokens, model), BF16),
        in_specs=[vmem] * 10 + [hbm] * 7,
        out_specs=vmem,
        scratch_shapes=[
            pltpu.VMEM((channels // group, rows + HALO, group), F32),
            pltpu.VMEM((rows + HALO, group), F32),
            pltpu.VMEM((taps.shape[0] + 1, channels), F32),
            pltpu.VMEM((HALO, channels), BF16),
            pltpu.VMEM((HALO, channels), BF16),
            pltpu.VMEM((rows, channels), BF16),
            pltpu.VMEM((tokens, channels), BF16),
            pltpu.VMEM((tokens, model), BF16),
            pltpu.VMEM((tokens, model), F32),
            pltpu.VMEM((tokens, model), BF16),
            pltpu.VMEM((2, tokens), jnp.int32),
            pltpu.VMEM((2, tokens), F32),
            pltpu.VMEM((rows, group), F32),
            pltpu.VMEM((near_slots, model), BF16),
            pltpu.VMEM((near_slots, model), BF16),
            pltpu.VMEM((2 * near_slots, model), BF16),
            pltpu.VMEM((2 * near_slots, model), BF16),
            pltpu.VMEM((near_slots, model), BF16),
            pltpu.VMEM((near_slots, model), BF16),
            pltpu.VMEM((tokens, model), BF16),
            pltpu.VMEM((tokens, model), BF16),
            pltpu.VMEM(conv_out.shape, BF16),
            pltpu.VMEM(expert_gate.shape, BF16),
            pltpu.VMEM(expert_up.shape, BF16),
            pltpu.VMEM(expert_down.shape, BF16),
            pltpu.VMEM(shared_gate.shape, BF16),
            pltpu.VMEM(shared_up.shape, BF16),
            pltpu.VMEM(shared_down.shape, BF16),
            dma((7,)),
            dma((4,)),
            dma((2,)),
            dma((n + n // 2,)),
            dma((n + n // 2,)),
            dma((n,)),
            dma((n,)),
            dma((10,)),
        ],
        compiler_params=pltpu.CompilerParams(
            collective_id=0, has_side_effects=True, vmem_limit_bytes=VMEM_LIMIT
        ),
    )(
        conv_value,
        conv_gate,
        taps,
        doc_ids[None, :],
        gn_gain[None, :],
        gn_shift[None, :],
        residual,
        norm_gain[None, :],
        routes.T,
        route_weight.T,
        conv_out,
        expert_gate,
        expert_up,
        expert_down,
        shared_gate,
        shared_up,
        shared_down,
    )


VMEM_LIMIT = 58 * 1024 * 1024


def fits(mesh):
    n = mesh.size
    return n & (n - 1) == 0 and n <= 32 and mesh.shape["tp"] == 2


def solution(mesh):
    return jax.shard_map(
        fused if fits(mesh) else per_device,
        mesh=mesh,
        in_specs=(
            P("sp", "tp"),
            P("sp", "tp"),
            P(None, "tp"),
            P("sp"),
            P("tp"),
            P("tp"),
            P(),
            P(("sp", "tp"), None),
            P(),
            P(("sp", "tp"), None),
            P(("sp", "tp"), None),
            P(("sp", "tp"), None, None),
            P(("sp", "tp"), None, None),
            P(("sp", "tp"), None, None),
            P(),
            P(),
            P(),
        ),
        out_specs=P(("sp", "tp"), None),
        check_vma=False,
    )
```

profile of v0, /device:TPU:1, one launch (start us, length us, event | category | flops | bytes accessed | tf_op | source)
XLA Modules:
  0.0 93.7 jit_solution(15131231311117716247)
XLA Ops:
  0.0 91.8 %shard_map.163 = bf16[128,2048]{1,0:T(8,128)(2,1)} custom-call(bf16[256,512]{1,0:T(8,128)(2,1)} %value_ref.1, bf16[256,512]{1,0:T(8,128)(2,1)} %gate_ref.1, bf16[31,512]{1,0:T(8,128)(2,1)} %taps_ref.1, s32[1,256]{1,0:T(1,128)} %bitcast.9, f32[1,512]{1,0:T(1,128)} %bitcast.7, f32[1,512]{1,0:T(1,128)} %bitcast.8, bf16[128,2048]{1,0:T(8,128)(2,1)} %resid_ref.1, ...), custom_call_target="tpu_custom_call" | custom-call | tf_op jit(solution)/shard_map/pallas_call | solution.py:570
  91.8 1.9 %copy.19 = bf16[128,2048]{1,0:T(8,128)(2,1)} copy(bf16[128,2048]{1,0:T(8,128)(2,1)} %shard_map.163) | data formatting | bytes 1048576
where the time goes:
time: 95.2 us; the launch traced here: 93.7 us
  Pallas kernels  91.8 us (96%)
  local copies, waits for them, and re-layouts  1.88 us (2%)
    pallas_call x1, Pallas kernels, fused(): pl.pallas_call(functools.partial(fused_kernel, n_sp, n_tp, capacity), out...  91.8 us

commit v1 on v0

v1 whole, which is shorter than its diff:
```python
import functools

import jax
import jax.numpy as jnp
from jax import lax
from jax.experimental import pallas as pl
from jax.experimental.pallas import tpu as pltpu
from jax.sharding import PartitionSpec as P

GROUPS = 8


epsilon = 1e-06


def from_behind(x, axis, by):
    peers = lax.axis_size(axis)
    pairs = [(i, i + by) for i in range(peers) if 0 <= i + by < peers]
    return lax.ppermute(x, axis, pairs)


def per_device(
    conv_value,
    conv_gate,
    taps,
    doc_ids,
    gn_gain,
    gn_shift,
    conv_out,
    residual,
    norm_gain,
    routes,
    route_weight,
    expert_gate,
    expert_up,
    expert_down,
    shared_gate,
    shared_up,
    shared_down,
):
    position_count, channel_count = conv_value.shape
    kernel_width = taps.shape[0]
    model_width = residual.shape[1]
    glu_out = (
        conv_value.astype(jnp.float32) * jax.nn.sigmoid(conv_gate.astype(jnp.float32))
    ).astype(jnp.bfloat16)
    rim_start = position_count - kernel_width + 1
    edge_glu, edge_ids = from_behind((glu_out[rim_start:], doc_ids[rim_start:]), "sp", 1)
    longer_glu = jnp.concatenate([edge_glu, glu_out], axis=0)
    longer_ids = jnp.concatenate([edge_ids, doc_ids], axis=0)
    conv_sum = jnp.zeros((position_count, channel_count), jnp.float32)
    for offset in range(kernel_width):
        same_doc = (longer_ids[offset : offset + position_count] == doc_ids)[:, None]
        tap_term = taps[offset].astype(jnp.float32)[None, :] * longer_glu[
            offset : offset + position_count
        ].astype(jnp.float32)
        conv_sum = conv_sum + jnp.where(same_doc, tap_term, 0.0)
    core_split = lax.axis_size("tp")
    groups_here = GROUPS // core_split
    grouped = conv_sum.reshape(position_count, groups_here, channel_count // groups_here)
    group_mean = jnp.mean(grouped, axis=-1, keepdims=True)
    centered = grouped - group_mean
    group_var = jnp.mean(centered * centered, axis=-1, keepdims=True)
    normalized = (centered * lax.rsqrt(group_var + epsilon)).reshape(position_count, channel_count)
    conv_act = jax.nn.silu(normalized * gn_gain + gn_shift).astype(jnp.bfloat16)
    token_rows = lax.all_to_all(conv_act, "tp", split_axis=0, concat_axis=1, tiled=True)
    projected = jnp.dot(token_rows, conv_out, preferred_element_type=jnp.float32)
    stream = (residual.astype(jnp.float32) + projected).astype(jnp.bfloat16)
    stream_wide = stream.astype(jnp.float32)
    normed = (
        stream_wide
        * lax.rsqrt(jnp.mean(stream_wide * stream_wide, axis=-1, keepdims=True) + epsilon)
        * norm_gain
    ).astype(jnp.bfloat16)
    token_count, top_count = routes.shape
    sequence_split = lax.axis_size("sp")
    device_count = sequence_split * core_split
    local_experts = expert_gate.shape[0]
    experts = local_experts * device_count
    capacity = 2 * token_count * top_count // experts
    flat_routes = routes.reshape(-1)
    onehot = (flat_routes[:, None] == jnp.arange(experts, dtype=jnp.int32)[None, :]).astype(
        jnp.int32
    )
    slot_index = jnp.sum(jnp.cumsum(onehot, axis=0) * onehot, axis=1) - 1
    target = flat_routes * capacity + slot_index
    source = (
        jnp.full((experts * capacity,), token_count, jnp.int32)
        .at[target]
        .set(jnp.arange(token_count * top_count, dtype=jnp.int32) // top_count)
    )
    padded_rows = jnp.concatenate([normed, jnp.zeros((1, model_width), normed.dtype)], axis=0)
    outgoing = padded_rows[source]
    shared_hidden = (
        jax.nn.silu(jnp.dot(normed, shared_gate, preferred_element_type=jnp.float32))
        * jnp.dot(normed, shared_up, preferred_element_type=jnp.float32)
    ).astype(jnp.bfloat16)
    shared_out = jnp.dot(shared_hidden, shared_down, preferred_element_type=jnp.float32)
    parcel = outgoing.reshape(device_count, local_experts, capacity, model_width)
    arrived = lax.all_to_all(parcel, ("sp", "tp"), split_axis=0, concat_axis=0, tiled=True)
    expert_rows = arrived[:, 0].reshape(-1, model_width)
    gate_part = jnp.dot(expert_rows, expert_gate[0], preferred_element_type=jnp.float32)
    up_part = jnp.dot(expert_rows, expert_up[0], preferred_element_type=jnp.float32)
    hidden = (jax.nn.silu(gate_part) * up_part).astype(jnp.bfloat16)
    result = jnp.dot(hidden, expert_down[0], preferred_element_type=jnp.float32).astype(
        jnp.bfloat16
    )
    results = [result.reshape(arrived.shape[0], arrived.shape[2], model_width)]
    returned = lax.all_to_all(
        jnp.stack(results, axis=1), ("sp", "tp"), split_axis=0, concat_axis=0, tiled=True
    )
    picked = returned.reshape(experts * capacity, model_width)[target].reshape(
        token_count, top_count, model_width
    )
    routed = jnp.zeros((token_count, model_width), jnp.float32)
    for route_index in range(top_count):
        routed = routed + route_weight[:, route_index, None] * picked[:, route_index].astype(
            jnp.float32
        )
    return (stream_wide + shared_out + routed).astype(jnp.bfloat16)


F32 = jnp.float32
BF16 = jnp.bfloat16
MESH_ID = pl.DeviceIdType.MESH
HALO = 32
CHUNK = 32
PLANES = 4
PARTS = 4
VMEM_LIMIT = 58 * 1024 * 1024


def flip(index, bits):
    out, weight = index, 1
    while weight <= bits:
        if (bits // weight) % 2:
            out = out + weight * (1 - 2 * ((index // weight) % 2))
        weight *= 2
    return out


def silu(v):
    return v / (1.0 + jnp.exp(-v))


ORDERS = {
    "E": (
        "P01", "D03", "D00", "P02", "P03", "T10", "S00", "P00", "P12", "T20", "P11", "D02",
        "D01", "T30", "X00", "P13", "P10", "P33", "P30", "X10", "P32", "M10", "P31", "P20",
        "M13", "P23", "X30", "M00", "M11", "M02", "M03", "P22", "M30", "P21", "M31", "M32",
        "X20", "M33", "M20", "M22", "M23", "M21", "F00", "M12", "M01", "F02", "F01", "F03",
    ),
    "I": (
        "D12", "D00", "D03", "P02", "D11", "P00", "D13", "R00", "T30", "L13", "L10", "D10",
        "P03", "T20", "L33", "P01", "L12", "P33", "L30", "L20", "D02", "T10", "X00", "L11",
        "P30", "P10", "D01", "L32", "L31", "P31", "P32", "L23", "P13", "L21", "P20", "P21",
        "P11", "S00", "P23", "P12", "L22", "P22", "X30", "M00", "X10", "M03", "M30", "M01",
        "M31", "M10", "M32", "X20", "M11", "M33", "M12", "M20", "M13", "M22", "M02", "M23",
        "M21", "F03", "F00", "F02", "F01",
    ),
}


def fused_kernel(n_sp, n_tp, capacity, *refs):
    hbm_in, out_hbm = refs[:17], refs[17]
    vmem_in = refs[18:35]
    (
        glu_ext,
        ids_ext,
        tap_rows,
        halo_send,
        halo_recv,
        act,
        act_recv,
        ids_here,
        base_ref,
        mail,
        picks,
        highs,
        lows,
        tok,
        outgoing,
        arrived,
        result,
        returned,
        partial,
        inc,
        out_ref,
        load_sem,
        halo_sem,
        act_sem,
        mail_send,
        mail_recv,
        tok_send,
        tok_recv,
        go_send,
        go_recv,
        back_send,
        back_recv,
        part_send,
        part_recv,
        out_sem,
    ) = refs[35:]
    (
        value_ref,
        gate_ref,
        taps_ref,
        ids_ref,
        gain_ref,
        shift_ref,
        resid_ref,
        ngain_ref,
        routes_ref,
        weight_ref,
        conv_out,
        sg,
        su,
        sd,
        eg,
        eu,
        ed,
    ) = vmem_in
    n = n_sp * n_tp
    per = n // PLANES
    sp, tp = lax.axis_index("sp"), lax.axis_index("tp")
    me = sp * n_tp + tp
    plane, here = me // per, me % per
    rows, channels = value_ref.shape
    tokens, model = resid_ref.shape
    width = taps_ref.shape[0]
    group = glu_ext.shape[2]
    groups = channels // group
    cols = model // PARTS
    slots = per * capacity
    side = 1 - 2 * (plane // 2)
    edge = plane % (PLANES - 1) == 0
    inner = plane % (PLANES - 1) != 0
    inner_count = (plane % (PLANES - 1) + 1) // 2

    def place(index):
        return (index // n_tp, index % n_tp)

    inward = place((plane + side) * per + here)
    outward = place((plane - side) * per + here)
    peers = [flip(here, k) for k in range(per - 1, 0, -1)]

    def peer_place(peer):
        return place(plane * per + peer)

    loads = [
        pltpu.make_async_copy(a, b, load_sem.at[i])
        for i, (a, b) in enumerate(zip(hbm_in, vmem_in))
    ]
    barrier = pltpu.get_barrier_semaphore()

    def greet(where):
        pl.semaphore_signal(barrier, inc=1, device_id=where, device_id_type=MESH_ID)

    for load in loads:
        load.start()
    for peer in peers:
        greet(peer_place(peer))
    greet(inward)

    @pl.when(inner)
    def _():
        greet(outward)

    @pl.when(sp < n_sp - 1)
    def _():
        greet((sp + 1, tp))

    @pl.when(sp > 0)
    def _():
        greet((sp - 1, tp))

    has_next = 1 - (sp + 1) // n_sp
    has_last = (sp + n_sp - 1) // n_sp
    for load in loads[:10]:
        load.wait()

    mail[0, 0:2, :] = routes_ref[...].astype(F32)
    mail[0, 2:4, :] = weight_ref[...]
    glu = (value_ref[...].astype(F32) * jax.nn.sigmoid(gate_ref[...].astype(F32))).astype(BF16)
    halo_send[...] = glu[rows - HALO :, :]
    for g in range(groups):
        glu_ext[g, pl.ds(HALO, rows), :] = glu[:, g * group : (g + 1) * group].astype(F32)
    for at in range(0, rows, group):
        row = ids_ref[:, at : at + group].astype(F32)
        column = jnp.broadcast_to(row, (group, group)).T
        ids_here[pl.ds(at, group), :] = column
        ids_ext[pl.ds(HALO + at, group), :] = column
    tap_rows[pl.ds(0, width), :] = taps_ref[...].astype(F32)

    def remote(src, dst, send_sem, recv_sem, where):
        return pltpu.make_async_remote_copy(
            src_ref=src,
            dst_ref=dst,
            send_sem=send_sem,
            recv_sem=recv_sem,
            device_id=where,
            device_id_type=MESH_ID,
        )

    halo_copies = [
        remote(halo_send, halo_recv, halo_sem.at[0], halo_sem.at[1], (sp + 1, tp)),
        remote(
            ids_here.at[pl.ds(rows - HALO, HALO)],
            ids_ext.at[pl.ds(0, HALO)],
            halo_sem.at[2],
            halo_sem.at[3],
            (sp + 1, tp),
        ),
    ]

    @pl.when(sp == 0)
    def _():
        glu_ext[:, pl.ds(0, HALO), :] = jnp.zeros((groups, HALO, group), F32)
        ids_ext[pl.ds(0, HALO), :] = jnp.full((HALO, group), -1.0, F32)

    def mail_copy(sent, landed, index, where):
        return remote(
            mail.at[sent], mail.at[landed], mail_send.at[index], mail_recv.at[landed], where
        )

    mail_edge = mail_copy(0, 1, 0, inward)
    mail_in = mail_copy(0, 2, 0, inward)
    mail_out = mail_copy(0, 1, 1, outward)
    mail_relay = [
        mail_copy(1, 3, 2, inward),
        mail_copy(2, 2, 3, outward),
        mail_copy(3, 3, 4, outward),
    ]

    other = (tp + 1) % n_tp
    theirs = pl.multiple_of(other * tokens, tokens)
    mine_at = pl.multiple_of(tp * tokens, tokens)
    act_copy = remote(
        act.at[pl.ds(theirs, tokens)], act_recv, act_sem.at[0], act_sem.at[1], (sp, other)
    )
    lot = tokens // CHUNK
    late = lot + 1

    def conv_step(i, carry):
        @pl.when(i == lot - 1)
        def _():
            pl.semaphore_wait(barrier, per - 1 + 1 + inner_count + has_next + has_last)

            @pl.when(sp < n_sp - 1)
            def _():
                for copy in halo_copies:
                    copy.start()

            @pl.when(edge)
            def _():
                mail_edge.start()

            @pl.when(inner)
            def _():
                mail_in.start()
                mail_out.start()

        @pl.when(i == late)
        def _():
            @pl.when(sp > 0)
            def _():
                for copy in halo_copies:
                    copy.wait_recv()
                for g in range(groups):
                    glu_ext[g, pl.ds(0, HALO), :] = halo_recv[
                        :, g * group : (g + 1) * group
                    ].astype(F32)

        low = (1 - i // lot) * (i + lot) + (i // lot) * (1 - i // late) + (i // (late + 1)) * (
            i - lot
        )
        high = (1 - i // late) * (i + 1) + (i // (late + 1)) * i
        r = pl.multiple_of(((1 - tp) * low + tp * high) * CHUNK, CHUNK)
        mine = ids_here[pl.ds(r, CHUNK), :]
        sums = [jnp.zeros((CHUNK, group), F32) for _ in range(groups)]
        for tap in range(width):
            off = HALO - width + 1 + tap
            same = ids_ext[pl.ds(r + off, CHUNK), :] == mine
            for g in range(groups):
                term = (
                    tap_rows[tap : tap + 1, g * group : (g + 1) * group]
                    * glu_ext[g, pl.ds(r + off, CHUNK), :]
                )
                sums[g] = sums[g] + jnp.where(same, term, 0.0)
        for g in range(groups):
            at = slice(g * group, (g + 1) * group)
            centered = sums[g] - jnp.mean(sums[g], axis=-1, keepdims=True)
            var = jnp.mean(centered * centered, axis=-1, keepdims=True)
            v = centered * lax.rsqrt(var + epsilon) * gain_ref[:, at] + shift_ref[:, at]
            act[pl.ds(r, CHUNK), at] = silu(v).astype(BF16)

        @pl.when((i == lot - 1) & (tp == 0))
        def _():
            act_copy.start()

        @pl.when((i == late) & (tp == 1))
        def _():
            act_copy.start()

        return carry

    lax.fori_loop(0, rows // CHUNK, conv_step, 0)

    @pl.when(inner)
    def _():
        mail_copy(1, 1, 0, inward).wait_recv()
        mail_relay[0].start()
        mail_copy(2, 2, 0, inward).wait_recv()
        mail_relay[1].start()

    loads[10].wait()
    projected = jnp.dot(
        act[pl.ds(mine_at, tokens), :],
        conv_out[pl.ds(pl.multiple_of(tp * channels, channels), channels), :],
        preferred_element_type=F32,
    )
    act_copy.wait_recv()
    projected = projected + jnp.dot(
        act_recv[...],
        conv_out[pl.ds(pl.multiple_of(other * channels, channels), channels), :],
        preferred_element_type=F32,
    )
    stream = (resid_ref[...].astype(F32) + projected).astype(BF16).astype(F32)
    base_ref[...] = stream
    normed = (
        stream
        * lax.rsqrt(jnp.mean(stream * stream, axis=-1, keepdims=True) + epsilon)
        * ngain_ref[...]
    ).astype(BF16)
    for q in range(PARTS):
        tok[0, q] = normed[:, q * cols : (q + 1) * cols]

    first = plane * per
    tri_r = lax.broadcasted_iota(jnp.int32, (tokens, tokens), 0)
    tri_c = lax.broadcasted_iota(jnp.int32, (tokens, tokens), 1)
    later = (tri_r < tri_c).astype(F32).astype(BF16)
    spread_t = (
        (
            lax.broadcasted_iota(jnp.int32, (slots, per), 0) // capacity
            == lax.broadcasted_iota(jnp.int32, (slots, per), 1)
        )
        .astype(F32)
        .astype(BF16)
    )
    row_slot = (lax.broadcasted_iota(jnp.int32, (slots, tokens), 0) % capacity).astype(F32)
    row_expert = (
        first + lax.broadcasted_iota(jnp.int32, (slots, tokens), 0) // capacity
    ).astype(F32)
    expert_row = (first + lax.broadcasted_iota(jnp.int32, (per, tokens), 0)).astype(F32)

    def tables(b):
        routes, weight = mail[b, 0:2, :], mail[b, 2:4, :]
        member = (
            (routes[0:1, :] == expert_row).astype(F32)
            + (routes[1:2, :] == expert_row).astype(F32)
        ).astype(BF16)
        slot = jnp.dot(member, later, preferred_element_type=F32).astype(BF16)
        right = jnp.dot(spread_t, slot, preferred_element_type=F32) == row_slot
        hit0 = jnp.where(right & (routes[0:1, :] == row_expert), 1.0, 0.0)
        hit1 = jnp.where(right & (routes[1:2, :] == row_expert), 1.0, 0.0)
        picks[b] = (hit0 + hit1).astype(BF16)
        mix = (hit0 * weight[0:1, :] + hit1 * weight[1:2, :]).T
        high = mix.astype(BF16)
        highs[b] = high
        lows[b] = (mix - high.astype(F32)).astype(BF16)

    def piece(index):
        return pl.ds(pl.multiple_of(index * capacity, capacity), capacity)

    most = pl.ds(0, (per - 1) * capacity)

    def tok_copy(sent, landed, index, q, where):
        return remote(
            tok.at[sent, q], tok.at[landed, q], tok_send.at[index, q], tok_recv.at[landed, q], where
        )

    def part_copy(b, landed, q, where):
        return remote(
            partial.at[b, q], inc.at[landed, q], part_send.at[b, q], part_recv.at[landed, q], where
        )

    def out_copy(q):
        return pltpu.make_async_copy(
            out_ref.at[q], out_hbm.at[:, pl.ds(q * cols, cols)], out_sem.at[q]
        )

    own_links = {
        "E": ((0, 1, 0, inward),),
        "I": ((0, 2, 0, inward), (0, 1, 1, outward)),
    }
    relays = {
        "E": {},
        "I": {1: (1, 3, 2, inward), 2: (2, 2, 3, outward), 3: (3, 3, 4, outward)},
    }
    part_links = {
        "E": {1: (0, inward), 2: (2, inward), 3: (3, inward)},
        "I": {1: (0, outward), 2: (1, inward), 3: (4, inward)},
    }
    joins = {"E": {1: None, 2: None, 3: None}, "I": {1: 4, 2: 2, 3: 3}}
    closes = {"E": (0,), "I": (0, 1)}

    def arrive(sem, buffer, b, q):
        area = buffer.at[b, q, most]
        remote(area, area, sem.at[b, q], sem.at[b, q], inward).wait_recv()

    def exchange(src, dst, sems, b, q):
        for peer in peers:
            remote(
                src.at[b, q, piece(peer)],
                dst.at[b, q, piece(here)],
                sems[0].at[b, q],
                sems[1].at[b, q],
                peer_place(peer),
            ).start()
        dst[b, q, piece(here), :] = src[b, q, piece(here), :]

    def op(role, kind, b, q):
        if kind == "D":
            for sent, landed, index, where in own_links[role][b : b + 1]:
                tok_copy(sent, landed, index, q, where).start()
        elif kind == "T":
            if role == "E":
                mail_copy(b, b, 0, inward).wait_recv()
            tables(b)
        elif kind == "R":
            mail_copy(3, 3, 0, inward).wait_recv()
            mail_relay[2].start()
        elif kind == "L":
            tok_copy(b, b, 0, q, inward).wait_recv()
            sent, landed, index, where = relays[role][b]
            tok_copy(sent, landed, index, q, where).start()
        elif kind == "P":
            if role == "E" and b:
                tok_copy(b, b, 0, q, inward).wait_recv()
            outgoing[b, q] = jnp.dot(picks[b], tok[b, q], preferred_element_type=F32).astype(BF16)
            exchange(outgoing, arrived, (go_send, go_recv), b, q)
        elif kind == "S":
            gate = jnp.zeros((tokens, sg.shape[1]), F32)
            up = jnp.zeros((tokens, sg.shape[1]), F32)
            for p in range(PARTS):
                k = slice(p * cols, (p + 1) * cols)
                gate = gate + jnp.dot(tok[0, p], sg[k, :], preferred_element_type=F32)
                up = up + jnp.dot(tok[0, p], su[k, :], preferred_element_type=F32)
            hidden = (silu(gate) * up).astype(BF16)
            base_ref[...] += jnp.dot(hidden, sd[...], preferred_element_type=F32)
        elif kind == "X":
            gate = jnp.zeros((slots, eg.shape[2]), F32)
            up = jnp.zeros((slots, eg.shape[2]), F32)
            for p in range(PARTS):
                k = slice(p * cols, (p + 1) * cols)
                arrive(go_recv, arrived, b, p)
                gate = gate + jnp.dot(arrived[b, p], eg[0, k, :], preferred_element_type=F32)
                up = up + jnp.dot(arrived[b, p], eu[0, k, :], preferred_element_type=F32)
            hidden = (silu(gate) * up).astype(BF16)
            for p in range(PARTS):
                k = slice(p * cols, (p + 1) * cols)
                result[b, p] = jnp.dot(
                    hidden, ed[0, :, k], preferred_element_type=F32
                ).astype(BF16)
                exchange(result, returned, (back_send, back_recv), b, p)
        elif kind == "M":
            arrive(back_recv, returned, b, q)
            back = returned[b, q]
            mixed = jnp.dot(highs[b], back, preferred_element_type=F32) + jnp.dot(
                lows[b], back, preferred_element_type=F32
            )
            if b == 0:
                base_ref[:, q * cols : (q + 1) * cols] += mixed
                return
            joined = joins[role][b]
            if joined is not None:
                part_copy(b, joined, q, inward).wait_recv()
                mixed = mixed + inc[joined, q].astype(F32)
            partial[b, q] = mixed.astype(BF16)
            landed, where = part_links[role][b]
            part_copy(b, landed, q, where).start()
        elif kind == "F":
            total = base_ref[:, q * cols : (q + 1) * cols]
            for joined in closes[role]:
                part_copy(1, joined, q, inward).wait_recv()
                total = total + inc[joined, q].astype(F32)
            out_ref[q] = total.astype(BF16)
            out_copy(q).start()

    def close(role):
        for sent, landed, index, where in own_links[role]:
            for q in range(PARTS):
                tok_copy(sent, landed, index, q, where).wait_send()
        for sent, landed, index, where in relays[role].values():
            for q in range(PARTS):
                tok_copy(sent, landed, index, q, where).wait_send()
        for b, (landed, where) in part_links[role].items():
            for q in range(PARTS):
                part_copy(b, landed, q, where).wait_send()

    tables(0)
    for load in loads[11:]:
        load.wait()
    for role, chosen in (("E", edge), ("I", inner)):

        @pl.when(chosen)
        def _(role=role):
            for step in ORDERS[role]:
                op(role, step[0], int(step[1]), int(step[2]))
            close(role)

    @pl.when(edge)
    def _():
        mail_edge.wait_send()

    @pl.when(inner)
    def _():
        mail_in.wait_send()
        mail_out.wait_send()
        for copy in mail_relay:
            copy.wait_send()

    act_copy.wait_send()

    @pl.when(sp < n_sp - 1)
    def _():
        for copy in halo_copies:
            copy.wait_send()

    for b in range(PLANES):
        for q in range(PARTS):
            for sem, buffer in ((go_send, outgoing), (back_send, result)):
                remote(
                    buffer.at[b, q, most], buffer.at[b, q, most], sem.at[b, q], sem.at[b, q], inward
                ).wait_send()
    for q in range(PARTS):
        out_copy(q).wait()


def fused(
    conv_value,
    conv_gate,
    taps,
    doc_ids,
    gn_gain,
    gn_shift,
    conv_out,
    residual,
    norm_gain,
    routes,
    route_weight,
    expert_gate,
    expert_up,
    expert_down,
    shared_gate,
    shared_up,
    shared_down,
):
    n_sp, n_tp = lax.axis_size("sp"), lax.axis_size("tp")
    n = n_sp * n_tp
    rows, channels = conv_value.shape
    tokens, model = residual.shape
    capacity = 2 * tokens * routes.shape[1] // n
    group = channels * n_tp // GROUPS
    slots = n // PLANES * capacity
    cols = model // PARTS
    operands = (
        conv_value,
        conv_gate,
        taps,
        doc_ids[None, :],
        gn_gain[None, :],
        gn_shift[None, :],
        residual,
        norm_gain[None, :],
        routes.T,
        route_weight.T,
        conv_out,
        shared_gate,
        shared_up,
        shared_down,
        expert_gate,
        expert_up,
        expert_down,
    )
    hbm = pl.BlockSpec(memory_space=pl.ANY)
    dma = pltpu.SemaphoreType.DMA
    return pl.pallas_call(
        functools.partial(fused_kernel, n_sp, n_tp, capacity),
        out_shape=jax.ShapeDtypeStruct((tokens, model), BF16),
        in_specs=[hbm] * len(operands),
        out_specs=hbm,
        scratch_shapes=[pltpu.VMEM(x.shape, x.dtype) for x in operands]
        + [
            pltpu.VMEM((channels // group, rows + HALO, group), F32),
            pltpu.VMEM((rows + HALO, group), F32),
            pltpu.VMEM((taps.shape[0] + 1, channels), F32),
            pltpu.VMEM((HALO, channels), BF16),
            pltpu.VMEM((HALO, channels), BF16),
            pltpu.VMEM((rows, channels), BF16),
            pltpu.VMEM((tokens, channels), BF16),
            pltpu.VMEM((rows, group), F32),
            pltpu.VMEM((tokens, model), F32),
            pltpu.VMEM((PLANES, 4, tokens), F32),
            pltpu.VMEM((PLANES, slots, tokens), BF16),
            pltpu.VMEM((PLANES, tokens, slots), BF16),
            pltpu.VMEM((PLANES, tokens, slots), BF16),
            pltpu.VMEM((PLANES, PARTS, tokens, cols), BF16),
            pltpu.VMEM((PLANES, PARTS, slots, cols), BF16),
            pltpu.VMEM((PLANES, PARTS, slots, cols), BF16),
            pltpu.VMEM((PLANES, PARTS, slots, cols), BF16),
            pltpu.VMEM((PLANES, PARTS, slots, cols), BF16),
            pltpu.VMEM((PLANES, PARTS, tokens, cols), BF16),
            pltpu.VMEM((5, PARTS, tokens, cols), BF16),
            pltpu.VMEM((PARTS, tokens, cols), BF16),
            dma((17,)),
            dma((4,)),
            dma((2,)),
            dma((5,)),
            dma((PLANES,)),
            dma((5, PARTS)),
            dma((PLANES, PARTS)),
            dma((PLANES, PARTS)),
            dma((PLANES, PARTS)),
            dma((PLANES, PARTS)),
            dma((PLANES, PARTS)),
            dma((PLANES, PARTS)),
            dma((5, PARTS)),
            dma((PARTS,)),
        ],
        compiler_params=pltpu.CompilerParams(
            collective_id=0, has_side_effects=True, vmem_limit_bytes=VMEM_LIMIT
        ),
    )(*operands)


def fits(mesh):
    n = mesh.size
    return n & (n - 1) == 0 and 8 < n <= 32 and mesh.shape["tp"] == 2


def solution(mesh):
    return jax.shard_map(
        fused if fits(mesh) else per_device,
        mesh=mesh,
        in_specs=(
            P("sp", "tp"),
            P("sp", "tp"),
            P(None, "tp"),
            P("sp"),
            P("tp"),
            P("tp"),
            P(),
            P(("sp", "tp"), None),
            P(),
            P(("sp", "tp"), None),
            P(("sp", "tp"), None),
            P(("sp", "tp"), None, None),
            P(("sp", "tp"), None, None),
            P(("sp", "tp"), None, None),
            P(),
            P(),
            P(),
        ),
        out_specs=P(("sp", "tp"), None),
        check_vma=False,
    )
```

time: 95.2 us -> 82.9 us (0.87)
  the two profiles are of different devices: /device:TPU:1 before, /device:TPU:8 now
where the time goes in v1:
time: 82.9 us; the launch traced here: 82.7 us
  Pallas kernels  80.9 us (98%)
  local copies, waits for them, and re-layouts  1.88 us (2%)
    pallas_call x1, Pallas kernels, fused(): pl.pallas_call(functools.partial(fused_kernel, n_sp, n_tp, capacity), out...  80.9 us
    unnamed x1, local copies, waits for them, and re-layouts  1.88 us

profile of v1, /device:TPU:8, one launch (start us, length us, event | category | flops | bytes accessed | tf_op | source)
XLA Modules:
  0.0 82.7 jit_solution(11794986127345153834)
XLA Ops:
  0.0 80.9 %shard_map.163 = bf16[128,2048]{1,0:T(8,128)(2,1)} custom-call(bf16[256,512]{1,0:T(8,128)(2,1)} %refs_0_.1, bf16[256,512]{1,0:T(8,128)(2,1)} %refs_1_.1, bf16[31,512]{1,0:T(8,128)(2,1)} %refs_2_.1, s32[1,256]{1,0:T(1,128)} %bitcast.9, f32[1,512]{1,0:T(1,128)} %bitcast.7, f32[1,512]{1,0:T(1,128)} %bitcast.8, bf16[128,2048]{1,0:T(8,128)(2,1)} %refs_6_.1, ...), custom_call_target="tpu_custom_call" | custom-call | tf_op jit(solution)/shard_map/pallas_call | solution.py:688
  80.9 1.9 %copy.19 = bf16[128,2048]{1,0:T(8,128)(2,1)} copy(bf16[128,2048]{1,0:T(8,128)(2,1)} %shard_map.163) | data formatting | bytes 1048576

commit v2 on v1

--- a/solution.py
+++ b/solution.py
@@ -145,24 +145,44 @@
 
 ORDERS = {
     "E": (
-        "P01", "D03", "D00", "P02", "P03", "T10", "S00", "P00", "P12", "T20", "P11", "D02",
-        "D01", "T30", "X00", "P13", "P10", "P33", "P30", "X10", "P32", "M10", "P31", "P20",
-        "M13", "P23", "X30", "M00", "M11", "M02", "M03", "P22", "M30", "P21", "M31", "M32",
-        "X20", "M33", "M20", "M22", "M23", "M21", "F00", "M12", "M01", "F02", "F01", "F03",
+        (
+            "D03", "T20", "D01", "T10", "D02", "P00", "P10", "P02", "D00", "P03", "P12", "P01",
+            "P11", "P13", "P22", "X00", "P20", "P23", "X10", "T30", "M03", "P31", "P21", "P33",
+            "X01", "M00", "S00", "M10", "P32", "P30", "M12", "X20", "M11", "M13", "M02", "M20",
+            "M21", "X30", "M23", "M22", "X31", "M30", "M32", "M33", "M31", "X21", "F00", "X11",
+            "F02", "M01", "F01", "F03",
+        ),
+        (
+            "P02", "D01", "P01", "P00", "T20", "P03", "D03", "X01", "X00", "T10", "D02", "T30",
+            "X10", "D00", "X20", "P31", "P30", "P33", "P32", "X30", "P23", "X31", "P21", "M03",
+            "P22", "M02", "M00", "P20", "S00", "P10", "M01", "M33", "P13", "P11", "M30", "P12",
+            "M31", "X21", "M32", "X11", "M20", "M23", "M22", "M21", "M13", "M10", "M12", "F02",
+            "M11", "F00", "F01", "F03",
+        ),
     ),
     "I": (
-        "D12", "D00", "D03", "P02", "D11", "P00", "D13", "R00", "T30", "L13", "L10", "D10",
-        "P03", "T20", "L33", "P01", "L12", "P33", "L30", "L20", "D02", "T10", "X00", "L11",
-        "P30", "P10", "D01", "L32", "L31", "P31", "P32", "L23", "P13", "L21", "P20", "P21",
-        "P11", "S00", "P23", "P12", "L22", "P22", "X30", "M00", "X10", "M03", "M30", "M01",
-        "M31", "M10", "M32", "X20", "M11", "M33", "M12", "M20", "M13", "M22", "M02", "M23",
-        "M21", "F03", "F00", "F02", "F01",
+        (
+            "D02", "D10", "P02", "D12", "D01", "D00", "D11", "T10", "D03", "P00", "L22", "T20",
+            "P01", "P22", "R00", "T30", "L13", "D13", "L21", "P13", "P03", "L11", "P11", "L20",
+            "P20", "X01", "L12", "L23", "L10", "X00", "L33", "S00", "P12", "P33", "L31", "L32",
+            "P23", "P10", "P21", "L30", "P30", "P32", "P31", "X20", "X30", "M20", "X10", "M21",
+            "M23", "M22", "M30", "X31", "M32", "M01", "M03", "M33", "X11", "M10", "M31", "F01",
+            "M02", "M12", "F02", "F03", "M00", "X21", "M13", "F00", "M11",
+        ),
+        (
+            "P00", "P03", "R00", "P01", "D01", "P02", "X01", "D03", "L21", "T10", "M02", "L11",
+            "L12", "L10", "D13", "T30", "L13", "D02", "P13", "M01", "L31", "X10", "T20", "L30",
+            "P30", "L33", "L32", "D12", "P33", "L23", "P31", "X20", "D00", "P32", "P21", "P10",
+            "X30", "D11", "X00", "P12", "D10", "L22", "S00", "L20", "P11", "P22", "P20", "P23",
+            "X31", "X11", "X21", "M30", "M33", "M32", "M31", "M10", "M13", "M12", "M20", "M23",
+            "M00", "M03", "M11", "M22", "M21", "F03", "F00", "F02", "F01",
+        ),
     ),
 }
 
 
 def fused_kernel(n_sp, n_tp, capacity, *refs):
-    hbm_in, out_hbm = refs[:17], refs[17]
+    hbm_in, out_ref = refs[:17], refs[17]
     vmem_in = refs[18:35]
     (
         glu_ext,
@@ -185,7 +205,9 @@
         returned,
         partial,
         inc,
-        out_ref,
+        gate_acc,
+        up_acc,
+        hidden_ref,
         load_sem,
         halo_sem,
         act_sem,
@@ -199,7 +221,6 @@
         back_recv,
         part_send,
         part_recv,
-        out_sem,
     ) = refs[35:]
     (
         value_ref,
@@ -339,10 +360,10 @@
         act.at[pl.ds(theirs, tokens)], act_recv, act_sem.at[0], act_sem.at[1], (sp, other)
     )
     lot = tokens // CHUNK
-    late = lot + 1
+    late = lot + 2
 
     def conv_step(i, carry):
-        @pl.when(i == lot - 1)
+        @pl.when(i == 0)
         def _():
             pl.semaphore_wait(barrier, per - 1 + 1 + inner_count + has_next + has_last)
 
@@ -371,8 +392,10 @@
                         :, g * group : (g + 1) * group
                     ].astype(F32)
 
-        low = (1 - i // lot) * (i + lot) + (i // lot) * (1 - i // late) + (i // (late + 1)) * (
-            i - lot
+        low = (
+            (1 - i // lot) * (i + lot)
+            + (i // lot) * (1 - i // late) * (i - lot + 1)
+            + (i // (late + 1)) * (i - lot)
         )
         high = (1 - i // late) * (i + 1) + (i // (late + 1)) * i
         r = pl.multiple_of(((1 - tp) * low + tp * high) * CHUNK, CHUNK)
@@ -426,7 +449,6 @@
         preferred_element_type=F32,
     )
     stream = (resid_ref[...].astype(F32) + projected).astype(BF16).astype(F32)
-    base_ref[...] = stream
     normed = (
         stream
         * lax.rsqrt(jnp.mean(stream * stream, axis=-1, keepdims=True) + epsilon)
@@ -434,6 +456,7 @@
     ).astype(BF16)
     for q in range(PARTS):
         tok[0, q] = normed[:, q * cols : (q + 1) * cols]
+        base_ref[q] = stream[:, q * cols : (q + 1) * cols]
 
     first = plane * per
     tri_r = lax.broadcasted_iota(jnp.int32, (tokens, tokens), 0)
@@ -472,7 +495,13 @@
     def piece(index):
         return pl.ds(pl.multiple_of(index * capacity, capacity), capacity)
 
-    most = pl.ds(0, (per - 1) * capacity)
+    chips = per // n_tp
+    lane = chips * capacity
+    chip = here // n_tp
+    mine_row = tp * chips + chip
+
+    def toward(sign):
+        return place((plane + side * sign) * per + here)
 
     def tok_copy(sent, landed, index, q, where):
         return remote(
@@ -484,45 +513,48 @@
             partial.at[b, q], inc.at[landed, q], part_send.at[b, q], part_recv.at[landed, q], where
         )
 
-    def out_copy(q):
-        return pltpu.make_async_copy(
-            out_ref.at[q], out_hbm.at[:, pl.ds(q * cols, cols)], out_sem.at[q]
-        )
-
-    own_links = {
-        "E": ((0, 1, 0, inward),),
-        "I": ((0, 2, 0, inward), (0, 1, 1, outward)),
-    }
-    relays = {
-        "E": {},
-        "I": {1: (1, 3, 2, inward), 2: (2, 2, 3, outward), 3: (3, 3, 4, outward)},
-    }
-    part_links = {
-        "E": {1: (0, inward), 2: (2, inward), 3: (3, inward)},
-        "I": {1: (0, outward), 2: (1, inward), 3: (4, inward)},
-    }
-    joins = {"E": {1: None, 2: None, 3: None}, "I": {1: 4, 2: 2, 3: 3}}
-    closes = {"E": (0,), "I": (0, 1)}
-
-    def arrive(sem, buffer, b, q):
-        area = buffer.at[b, q, most]
-        remote(area, area, sem.at[b, q], sem.at[b, q], inward).wait_recv()
-
-    def exchange(src, dst, sems, b, q):
+    def bytes_of(buffer, b, q, count, sem):
+        area = buffer.at[b, q, pl.ds(0, count * capacity)]
+        return remote(area, area, sem, sem, inward)
+
+    def send_rows(core, b, q):
         for peer in peers:
             remote(
-                src.at[b, q, piece(peer)],
-                dst.at[b, q, piece(here)],
-                sems[0].at[b, q],
-                sems[1].at[b, q],
+                outgoing.at[b, q, piece(peer)],
+                arrived.at[b, q, piece(mine_row)],
+                go_send.at[b, q],
+                go_recv.at[b, q, core],
                 peer_place(peer),
             ).start()
-        dst[b, q, piece(here), :] = src[b, q, piece(here), :]
-
-    def op(role, kind, b, q):
+        arrived[b, q, piece(mine_row), :] = outgoing[b, q, piece(here), :]
+
+    def return_rows(core, b, q, s):
+        for apart in range(chips - 1, -1, -1):
+            target = flip(chip, apart)
+            if apart == 0 and s == core:
+                returned[b, q, piece(here), :] = result[b, q, piece(mine_row), :]
+            else:
+                remote(
+                    result.at[b, q, piece(s * chips + target)],
+                    returned.at[b, q, piece(here)],
+                    back_send.at[b, q],
+                    back_recv.at[b, q],
+                    peer_place(target * n_tp + s),
+                ).start()
+
+    landing = {"E": {0: (1, 1)}, "I": {0: (2, 1), 1: (1, -1)}}
+    relaying = {1: (3, 2, 1), 2: (2, 3, -1), 3: (3, 4, -1)}
+    part_to = {
+        "E": {1: (0, 1), 2: (2, 1), 3: (3, 1)},
+        "I": {1: (0, -1), 2: (1, 1), 3: (4, 1)},
+    }
+    joins = {1: 4, 2: 2, 3: 3}
+    closes = {"E": (0,), "I": (0, 1)}
+
+    def op(role, core, kind, b, q):
         if kind == "D":
-            for sent, landed, index, where in own_links[role][b : b + 1]:
-                tok_copy(sent, landed, index, q, where).start()
+            landed, sign = landing[role][b]
+            tok_copy(0, landed, b, q, toward(sign)).start()
         elif kind == "T":
             if role == "E":
                 mail_copy(b, b, 0, inward).wait_recv()
@@ -532,13 +564,13 @@
             mail_relay[2].start()
         elif kind == "L":
             tok_copy(b, b, 0, q, inward).wait_recv()
-            sent, landed, index, where = relays[role][b]
-            tok_copy(sent, landed, index, q, where).start()
+            landed, index, sign = relaying[b]
+            tok_copy(b, landed, index, q, toward(sign)).start()
         elif kind == "P":
             if role == "E" and b:
                 tok_copy(b, b, 0, q, inward).wait_recv()
             outgoing[b, q] = jnp.dot(picks[b], tok[b, q], preferred_element_type=F32).astype(BF16)
-            exchange(outgoing, arrived, (go_send, go_recv), b, q)
+            send_rows(core, b, q)
         elif kind == "S":
             gate = jnp.zeros((tokens, sg.shape[1]), F32)
             up = jnp.zeros((tokens, sg.shape[1]), F32)
@@ -547,67 +579,81 @@
                 gate = gate + jnp.dot(tok[0, p], sg[k, :], preferred_element_type=F32)
                 up = up + jnp.dot(tok[0, p], su[k, :], preferred_element_type=F32)
             hidden = (silu(gate) * up).astype(BF16)
-            base_ref[...] += jnp.dot(hidden, sd[...], preferred_element_type=F32)
-        elif kind == "X":
-            gate = jnp.zeros((slots, eg.shape[2]), F32)
-            up = jnp.zeros((slots, eg.shape[2]), F32)
             for p in range(PARTS):
                 k = slice(p * cols, (p + 1) * cols)
-                arrive(go_recv, arrived, b, p)
-                gate = gate + jnp.dot(arrived[b, p], eg[0, k, :], preferred_element_type=F32)
-                up = up + jnp.dot(arrived[b, p], eu[0, k, :], preferred_element_type=F32)
-            hidden = (silu(gate) * up).astype(BF16)
-            for p in range(PARTS):
-                k = slice(p * cols, (p + 1) * cols)
-                result[b, p] = jnp.dot(
-                    hidden, ed[0, :, k], preferred_element_type=F32
+                base_ref[p] += jnp.dot(hidden, sd[:, k], preferred_element_type=F32)
+        elif kind == "X":
+            s, at = q, slice(q * lane, (q + 1) * lane)
+            count = chips - int(s == core)
+            gate_acc[...] = jnp.zeros((lane, eg.shape[2]), F32)
+            up_acc[...] = jnp.zeros((lane, eg.shape[2]), F32)
+
+            def widen(p, carry):
+                k = pl.ds(pl.multiple_of(p * cols, cols), cols)
+                bytes_of(arrived, b, p, count, go_recv.at[b, p, s]).wait_recv()
+                x = arrived[b, p, at, :]
+                gate_acc[...] += jnp.dot(x, eg[0, k, :], preferred_element_type=F32)
+                up_acc[...] += jnp.dot(x, eu[0, k, :], preferred_element_type=F32)
+                return carry
+
+            lax.fori_loop(0, PARTS, widen, 0, unroll=2)
+            hidden_ref[...] = (silu(gate_acc[...]) * up_acc[...]).astype(BF16)
+
+            def narrow(p, carry):
+                k = pl.ds(pl.multiple_of(p * cols, cols), cols)
+                result[b, p, at, :] = jnp.dot(
+                    hidden_ref[...], ed[0, :, k], preferred_element_type=F32
                 ).astype(BF16)
-                exchange(result, returned, (back_send, back_recv), b, p)
+                return_rows(core, b, p, s)
+                return carry
+
+            lax.fori_loop(0, PARTS, narrow, 0, unroll=2)
         elif kind == "M":
-            arrive(back_recv, returned, b, q)
+            bytes_of(returned, b, q, per - 1, back_recv.at[b, q]).wait_recv()
             back = returned[b, q]
             mixed = jnp.dot(highs[b], back, preferred_element_type=F32) + jnp.dot(
                 lows[b], back, preferred_element_type=F32
             )
             if b == 0:
-                base_ref[:, q * cols : (q + 1) * cols] += mixed
+                base_ref[q] += mixed
                 return
-            joined = joins[role][b]
-            if joined is not None:
+            if role == "I":
+                joined = joins[b]
                 part_copy(b, joined, q, inward).wait_recv()
                 mixed = mixed + inc[joined, q].astype(F32)
             partial[b, q] = mixed.astype(BF16)
-            landed, where = part_links[role][b]
-            part_copy(b, landed, q, where).start()
+            landed, sign = part_to[role][b]
+            part_copy(b, landed, q, toward(sign)).start()
         elif kind == "F":
-            total = base_ref[:, q * cols : (q + 1) * cols]
+            total = base_ref[q]
             for joined in closes[role]:
                 part_copy(1, joined, q, inward).wait_recv()
                 total = total + inc[joined, q].astype(F32)
-            out_ref[q] = total.astype(BF16)
-            out_copy(q).start()
+            out_ref[:, q * cols : (q + 1) * cols] = total.astype(BF16)
 
     def close(role):
-        for sent, landed, index, where in own_links[role]:
+        for index, (landed, sign) in landing[role].items():
             for q in range(PARTS):
-                tok_copy(sent, landed, index, q, where).wait_send()
-        for sent, landed, index, where in relays[role].values():
+                tok_copy(0, landed, index, q, toward(sign)).wait_send()
+        for b, (landed, index, sign) in relaying.items():
+            if role == "I":
+                for q in range(PARTS):
+                    tok_copy(b, landed, index, q, toward(sign)).wait_send()
+        for b, (landed, sign) in part_to[role].items():
             for q in range(PARTS):
-                tok_copy(sent, landed, index, q, where).wait_send()
-        for b, (landed, where) in part_links[role].items():
-            for q in range(PARTS):
-                part_copy(b, landed, q, where).wait_send()
+                part_copy(b, landed, q, toward(sign)).wait_send()
 
     tables(0)
     for load in loads[11:]:
         load.wait()
     for role, chosen in (("E", edge), ("I", inner)):
-
-        @pl.when(chosen)
-        def _(role=role):
-            for step in ORDERS[role]:
-                op(role, step[0], int(step[1]), int(step[2]))
-            close(role)
+        for core in range(n_tp):
+
+            @pl.when(chosen & (tp == core))
+            def _(role=role, core=core):
+                for step in ORDERS[role][core]:
+                    op(role, core, step[0], int(step[1]), int(step[2]))
+                close(role)
 
     @pl.when(edge)
     def _():
@@ -629,12 +675,8 @@
 
     for b in range(PLANES):
         for q in range(PARTS):
-            for sem, buffer in ((go_send, outgoing), (back_send, result)):
-                remote(
-                    buffer.at[b, q, most], buffer.at[b, q, most], sem.at[b, q], sem.at[b, q], inward
-                ).wait_send()
-    for q in range(PARTS):
-        out_copy(q).wait()
+            bytes_of(outgoing, b, q, per - 1, go_send.at[b, q]).wait_send()
+            bytes_of(result, b, q, per - 1, back_send.at[b, q]).wait_send()
 
 
 def fused(
@@ -687,9 +729,9 @@
     dma = pltpu.SemaphoreType.DMA
     return pl.pallas_call(
         functools.partial(fused_kernel, n_sp, n_tp, capacity),
-        out_shape=jax.ShapeDtypeStruct((tokens, model), BF16),
+        out_shape=pltpu.VMEM((tokens, model), BF16),
         in_specs=[hbm] * len(operands),
-        out_specs=hbm,
+        out_specs=pl.BlockSpec(memory_space=pltpu.VMEM),
         scratch_shapes=[pltpu.VMEM(x.shape, x.dtype) for x in operands]
         + [
             pltpu.VMEM((channels // group, rows + HALO, group), F32),
@@ -700,7 +742,7 @@
             pltpu.VMEM((rows, channels), BF16),
             pltpu.VMEM((tokens, channels), BF16),
             pltpu.VMEM((rows, group), F32),
-            pltpu.VMEM((tokens, model), F32),
+            pltpu.VMEM((PARTS, tokens, cols), F32),
             pltpu.VMEM((PLANES, 4, tokens), F32),
             pltpu.VMEM((PLANES, slots, tokens), BF16),
             pltpu.VMEM((PLANES, tokens, slots), BF16),
@@ -712,7 +754,9 @@
             pltpu.VMEM((PLANES, PARTS, slots, cols), BF16),
             pltpu.VMEM((PLANES, PARTS, tokens, cols), BF16),
             pltpu.VMEM((5, PARTS, tokens, cols), BF16),
-            pltpu.VMEM((PARTS, tokens, cols), BF16),
+            pltpu.VMEM((slots // n_tp, expert_gate.shape[2]), F32),
+            pltpu.VMEM((slots // n_tp, expert_gate.shape[2]), F32),
+            pltpu.VMEM((slots // n_tp, expert_gate.shape[2]), BF16),
             dma((17,)),
             dma((4,)),
             dma((2,)),
@@ -721,12 +765,11 @@
             dma((5, PARTS)),
             dma((PLANES, PARTS)),
             dma((PLANES, PARTS)),
-            dma((PLANES, PARTS)),
+            dma((PLANES, PARTS, n_tp)),
             dma((PLANES, PARTS)),
             dma((PLANES, PARTS)),
             dma((PLANES, PARTS)),
             dma((5, PARTS)),
-            dma((PARTS,)),
         ],
         compiler_params=pltpu.CompilerParams(
             collective_id=0, has_side_effects=True, vmem_limit_bytes=VMEM_LIMIT

time: 82.9 us -> 72.8 us (0.88)
  the two profiles are of different devices: /device:TPU:8 before, /device:TPU:1 now
where the time goes in v2:
time: 72.8 us; the launch traced here: 72.7 us
  Pallas kernels  71.9 us (99%)
  local copies, waits for them, and re-layouts  0.8 us (1%)
    pallas_call x1, Pallas kernels, fused(): pl.pallas_call(functools.partial(fused_kernel, n_sp, n_tp, capacity), out...  71.9 us

profile of v2, /device:TPU:1, one launch (start us, length us, event | category | flops | bytes accessed | tf_op | source)
XLA Modules:
  0.0 72.7 jit_solution(9492920667932569933)
XLA Ops:
  0.0 71.9 %shard_map.163 = bf16[128,2048]{1,0:T(8,128)(2,1)S(1)} custom-call(bf16[256,512]{1,0:T(8,128)(2,1)} %refs_0_.1, bf16[256,512]{1,0:T(8,128)(2,1)} %refs_1_.1, bf16[31,512]{1,0:T(8,128)(2,1)} %refs_2_.1, s32[1,256]{1,0:T(1,128)} %bitcast.9, f32[1,512]{1,0:T(1,128)} %bitcast.7, f32[1,512]{1,0:T(1,128)} %bitcast.8, bf16[128,2048]{1,0:T(8,128)(2,1)} %refs_6_.1, ...), custom_call_target="tpu_custom_call" | custom-call | tf_op jit(solution)/shard_map/pallas_call | solution.py:730
  71.9 0.8 %copy.19 = bf16[128,2048]{1,0:T(8,128)(2,1)} copy(bf16[128,2048]{1,0:T(8,128)(2,1)S(1)} %shard_map.163) | data formatting | bytes 1048576

commit v3 on v2

--- a/solution.py
+++ b/solution.py
@@ -146,36 +146,36 @@
 ORDERS = {
     "E": (
         (
-            "D03", "T20", "D01", "T10", "D02", "P00", "P10", "P02", "D00", "P03", "P12", "P01",
-            "P11", "P13", "P22", "X00", "P20", "P23", "X10", "T30", "M03", "P31", "P21", "P33",
-            "X01", "M00", "S00", "M10", "P32", "P30", "M12", "X20", "M11", "M13", "M02", "M20",
-            "M21", "X30", "M23", "M22", "X31", "M30", "M32", "M33", "M31", "X21", "F00", "X11",
-            "F02", "M01", "F01", "F03",
+            "P02", "P03", "P00", "T20", "D00", "P01", "T10", "D02", "D03", "P11", "D01", "P13",
+            "P12", "T30", "P10", "X00", "P20", "P21", "P23", "P22", "X10", "P30", "P32", "P33",
+            "P31", "M00", "M10", "X20", "M11", "M12", "X30", "M20", "M01", "M22", "M02", "M21",
+            "S00", "M23", "X01", "M30", "M33", "M32", "M03", "M31", "X31", "M13", "X21", "F03",
+            "X11", "F01", "F00", "F02",
         ),
         (
-            "P02", "D01", "P01", "P00", "T20", "P03", "D03", "X01", "X00", "T10", "D02", "T30",
-            "X10", "D00", "X20", "P31", "P30", "P33", "P32", "X30", "P23", "X31", "P21", "M03",
-            "P22", "M02", "M00", "P20", "S00", "P10", "M01", "M33", "P13", "P11", "M30", "P12",
-            "M31", "X21", "M32", "X11", "M20", "M23", "M22", "M21", "M13", "M10", "M12", "F02",
-            "M11", "F00", "F01", "F03",
+            "D02", "T20", "S00", "T10", "P00", "P03", "P02", "X00", "D01", "T30", "P01", "D00",
+            "X10", "D03", "X20", "P30", "P31", "X30", "P33", "P32", "X01", "P22", "P20", "X31",
+            "P23", "P21", "M30", "P12", "M02", "P10", "P11", "M32", "M33", "P13", "X21", "M31",
+            "M20", "M00", "M21", "X11", "M22", "M03", "M23", "M10", "M01", "M13", "M12", "F00",
+            "F02", "F03", "M11", "F01",
         ),
     ),
     "I": (
         (
-            "D02", "D10", "P02", "D12", "D01", "D00", "D11", "T10", "D03", "P00", "L22", "T20",
-            "P01", "P22", "R00", "T30", "L13", "D13", "L21", "P13", "P03", "L11", "P11", "L20",
-            "P20", "X01", "L12", "L23", "L10", "X00", "L33", "S00", "P12", "P33", "L31", "L32",
-            "P23", "P10", "P21", "L30", "P30", "P32", "P31", "X20", "X30", "M20", "X10", "M21",
-            "M23", "M22", "M30", "X31", "M32", "M01", "M03", "M33", "X11", "M10", "M31", "F01",
-            "M02", "M12", "F02", "F03", "M00", "X21", "M13", "F00", "M11",
+            "D01", "D11", "D13", "D12", "S00", "P03", "D00", "P01", "R00", "D02", "T30", "P02",
+            "T10", "D10", "T20", "L21", "P00", "D03", "L10", "P21", "L12", "L20", "P12", "P10",
+            "P20", "L23", "L13", "L22", "P22", "L32", "L11", "L30", "P13", "X01", "P32", "P11",
+            "L33", "P23", "P30", "P33", "L31", "P31", "X00", "X20", "X10", "X30", "M20", "M22",
+            "M21", "M23", "M01", "M30", "M02", "M33", "X31", "M32", "M03", "M00", "M10", "M31",
+            "F02", "M13", "X11", "M12", "F00", "M11", "X21", "F03", "F01",
         ),
         (
-            "P00", "P03", "R00", "P01", "D01", "P02", "X01", "D03", "L21", "T10", "M02", "L11",
-            "L12", "L10", "D13", "T30", "L13", "D02", "P13", "M01", "L31", "X10", "T20", "L30",
-            "P30", "L33", "L32", "D12", "P33", "L23", "P31", "X20", "D00", "P32", "P21", "P10",
-            "X30", "D11", "X00", "P12", "D10", "L22", "S00", "L20", "P11", "P22", "P20", "P23",
-            "X31", "X11", "X21", "M30", "M33", "M32", "M31", "M10", "M13", "M12", "M20", "M23",
-            "M00", "M03", "M11", "M22", "M21", "F03", "F00", "F02", "F01",
+            "P02", "R00", "T10", "P03", "P00", "P01", "T20", "X00", "T30", "L12", "L10", "S00",
+            "L11", "D02", "P12", "L13", "D00", "D03", "L30", "P10", "P11", "L31", "P13", "X20",
+            "D01", "L32", "L33", "P31", "P32", "L20", "P30", "L22", "P33", "L21", "X30", "D10",
+            "P20", "X10", "L23", "P22", "D12", "P23", "D11", "D13", "P21", "X01", "X31", "X11",
+            "X21", "M30", "M32", "M33", "M03", "M10", "M31", "M00", "M12", "M13", "M20", "M21",
+            "M11", "M02", "M22", "M23", "F00", "F02", "F03", "M01", "F01",
         ),
     ),
 }
@@ -362,6 +362,40 @@
     lot = tokens // CHUNK
     late = lot + 2
 
+    first = plane * per
+    tri_r = lax.broadcasted_iota(jnp.int32, (tokens, tokens), 0)
+    tri_c = lax.broadcasted_iota(jnp.int32, (tokens, tokens), 1)
+    later = (tri_r < tri_c).astype(F32).astype(BF16)
+    spread_t = (
+        (
+            lax.broadcasted_iota(jnp.int32, (slots, per), 0) // capacity
+            == lax.broadcasted_iota(jnp.int32, (slots, per), 1)
+        )
+        .astype(F32)
+        .astype(BF16)
+    )
+    row_slot = (lax.broadcasted_iota(jnp.int32, (slots, tokens), 0) % capacity).astype(F32)
+    row_expert = (
+        first + lax.broadcasted_iota(jnp.int32, (slots, tokens), 0) // capacity
+    ).astype(F32)
+    expert_row = (first + lax.broadcasted_iota(jnp.int32, (per, tokens), 0)).astype(F32)
+
+    def tables(b):
+        routes, weight = mail[b, 0:2, :], mail[b, 2:4, :]
+        member = (
+            (routes[0:1, :] == expert_row).astype(F32)
+            + (routes[1:2, :] == expert_row).astype(F32)
+        ).astype(BF16)
+        slot = jnp.dot(member, later, preferred_element_type=F32).astype(BF16)
+        right = jnp.dot(spread_t, slot, preferred_element_type=F32) == row_slot
+        hit0 = jnp.where(right & (routes[0:1, :] == row_expert), 1.0, 0.0)
+        hit1 = jnp.where(right & (routes[1:2, :] == row_expert), 1.0, 0.0)
+        picks[b] = (hit0 + hit1).astype(BF16)
+        mix = (hit0 * weight[0:1, :] + hit1 * weight[1:2, :]).T
+        high = mix.astype(BF16)
+        highs[b] = high
+        lows[b] = (mix - high.astype(F32)).astype(BF16)
+
     def conv_step(i, carry):
         @pl.when(i == 0)
         def _():
@@ -383,6 +417,8 @@
 
         @pl.when(i == late)
         def _():
+            tables(0)
+
             @pl.when(sp > 0)
             def _():
                 for copy in halo_copies:
@@ -457,40 +493,6 @@
     for q in range(PARTS):
         tok[0, q] = normed[:, q * cols : (q + 1) * cols]
         base_ref[q] = stream[:, q * cols : (q + 1) * cols]
-
-    first = plane * per
-    tri_r = lax.broadcasted_iota(jnp.int32, (tokens, tokens), 0)
-    tri_c = lax.broadcasted_iota(jnp.int32, (tokens, tokens), 1)
-    later = (tri_r < tri_c).astype(F32).astype(BF16)
-    spread_t = (
-        (
-            lax.broadcasted_iota(jnp.int32, (slots, per), 0) // capacity
-            == lax.broadcasted_iota(jnp.int32, (slots, per), 1)
-        )
-        .astype(F32)
-        .astype(BF16)
-    )
-    row_slot = (lax.broadcasted_iota(jnp.int32, (slots, tokens), 0) % capacity).astype(F32)
-    row_expert = (
-        first + lax.broadcasted_iota(jnp.int32, (slots, tokens), 0) // capacity
-    ).astype(F32)
-    expert_row = (first + lax.broadcasted_iota(jnp.int32, (per, tokens), 0)).astype(F32)
-
-    def tables(b):
-        routes, weight = mail[b, 0:2, :], mail[b, 2:4, :]
-        member = (
-            (routes[0:1, :] == expert_row).astype(F32)
-            + (routes[1:2, :] == expert_row).astype(F32)
-        ).astype(BF16)
-        slot = jnp.dot(member, later, preferred_element_type=F32).astype(BF16)
-        right = jnp.dot(spread_t, slot, preferred_element_type=F32) == row_slot
-        hit0 = jnp.where(right & (routes[0:1, :] == row_expert), 1.0, 0.0)
-        hit1 = jnp.where(right & (routes[1:2, :] == row_expert), 1.0, 0.0)
-        picks[b] = (hit0 + hit1).astype(BF16)
-        mix = (hit0 * weight[0:1, :] + hit1 * weight[1:2, :]).T
-        high = mix.astype(BF16)
-        highs[b] = high
-        lows[b] = (mix - high.astype(F32)).astype(BF16)
 
     def piece(index):
         return pl.ds(pl.multiple_of(index * capacity, capacity), capacity)
@@ -643,11 +645,10 @@
             for q in range(PARTS):
                 part_copy(b, landed, q, toward(sign)).wait_send()
 
-    tables(0)
     for load in loads[11:]:
         load.wait()
-    for role, chosen in (("E", edge), ("I", inner)):
-        for core in range(n_tp):
+    for core in range(n_tp):
+        for role, chosen in (("E", edge), ("I", inner)):
 
             @pl.when(chosen & (tp == core))
             def _(role=role, core=core):

time: 72.8 us -> 71.2 us (0.978)
  Pallas kernels: 71.9 us -> 69.6 us
    pallas_call x1, Pallas kernels: 71.9 us -> 69.6 us  [fused(): pl.pallas_call(functools.partial(fused_kernel, n_sp, n_tp, capacity), out...]
where the time goes in v3:
time: 71.2 us; the launch traced here: 70.4 us
  Pallas kernels  69.6 us (98%)
  local copies, waits for them, and re-layouts  0.8 us (1%)
    pallas_call x1, Pallas kernels, fused(): pl.pallas_call(functools.partial(fused_kernel, n_sp, n_tp, capacity), out...  69.6 us

profile of v3, /device:TPU:1, one launch (start us, length us, event | category | flops | bytes accessed | tf_op | source)
XLA Modules:
  0.0 70.4 jit_solution(4862428342715986325)
XLA Ops:
  0.0 69.6 %shard_map.163 = bf16[128,2048]{1,0:T(8,128)(2,1)S(1)} custom-call(bf16[256,512]{1,0:T(8,128)(2,1)} %refs_0_.1, bf16[256,512]{1,0:T(8,128)(2,1)} %refs_1_.1, bf16[31,512]{1,0:T(8,128)(2,1)} %refs_2_.1, s32[1,256]{1,0:T(1,128)} %bitcast.9, f32[1,512]{1,0:T(1,128)} %bitcast.7, f32[1,512]{1,0:T(1,128)} %bitcast.8, bf16[128,2048]{1,0:T(8,128)(2,1)} %refs_6_.1, ...), custom_call_target="tpu_custom_call" | custom-call | tf_op jit(solution)/shard_map/pallas_call | solution.py:731
  69.6 0.8 %copy.19 = bf16[128,2048]{1,0:T(8,128)(2,1)} copy(bf16[128,2048]{1,0:T(8,128)(2,1)S(1)} %shard_map.163) | data formatting | bytes 1048576

commit v4 on v3

--- a/solution.py
+++ b/solution.py
@@ -146,36 +146,36 @@
 ORDERS = {
     "E": (
         (
-            "P02", "P03", "P00", "T20", "D00", "P01", "T10", "D02", "D03", "P11", "D01", "P13",
-            "P12", "T30", "P10", "X00", "P20", "P21", "P23", "P22", "X10", "P30", "P32", "P33",
-            "P31", "M00", "M10", "X20", "M11", "M12", "X30", "M20", "M01", "M22", "M02", "M21",
-            "S00", "M23", "X01", "M30", "M33", "M32", "M03", "M31", "X31", "M13", "X21", "F03",
-            "X11", "F01", "F00", "F02",
+            "D00", "T20", "P03", "P02", "P00", "X01", "D02", "D03", "D01", "P01", "X11", "T30",
+            "X21", "S00", "P32", "P22", "P31", "T10", "P30", "P33", "X31", "P21", "P20", "P23",
+            "X30", "P12", "P10", "P11", "M31", "M33", "M32", "P13", "X20", "X00", "M30", "M20",
+            "M21", "X10", "M23", "M22", "M01", "M02", "M10", "F01", "M03", "M00", "M13", "F03",
+            "M12", "M11", "F02", "F00",
         ),
         (
-            "D02", "T20", "S00", "T10", "P00", "P03", "P02", "X00", "D01", "T30", "P01", "D00",
-            "X10", "D03", "X20", "P30", "P31", "X30", "P33", "P32", "X01", "P22", "P20", "X31",
-            "P23", "P21", "M30", "P12", "M02", "P10", "P11", "M32", "M33", "P13", "X21", "M31",
-            "M20", "M00", "M21", "X11", "M22", "M03", "M23", "M10", "M01", "M13", "M12", "F00",
-            "F02", "F03", "M11", "F01",
+            "P02", "P03", "P00", "D03", "D01", "D00", "P01", "T20", "T10", "D02", "P10", "P13",
+            "P12", "P11", "P22", "P20", "T30", "P21", "P23", "X01", "P33", "X21", "X11", "M02",
+            "P30", "M01", "M03", "M20", "P32", "P31", "M22", "M21", "M12", "M11", "M23", "M13",
+            "X31", "M30", "M31", "X30", "M32", "S00", "M33", "X00", "X20", "M10", "X10", "M00",
+            "F00", "F01", "F02", "F03",
         ),
     ),
     "I": (
         (
-            "D01", "D11", "D13", "D12", "S00", "P03", "D00", "P01", "R00", "D02", "T30", "P02",
-            "T10", "D10", "T20", "L21", "P00", "D03", "L10", "P21", "L12", "L20", "P12", "P10",
-            "P20", "L23", "L13", "L22", "P22", "L32", "L11", "L30", "P13", "X01", "P32", "P11",
-            "L33", "P23", "P30", "P33", "L31", "P31", "X00", "X20", "X10", "X30", "M20", "M22",
-            "M21", "M23", "M01", "M30", "M02", "M33", "X31", "M32", "M03", "M00", "M10", "M31",
-            "F02", "M13", "X11", "M12", "F00", "M11", "X21", "F03", "F01",
+            "P02", "P03", "P01", "T10", "L10", "P00", "R00", "T20", "L12", "T30", "P12", "D02",
+            "X00", "L11", "L30", "S00", "L13", "L22", "L32", "D03", "L31", "D01", "L33", "P13",
+            "D00", "X01", "P31", "M02", "L21", "L23", "M00", "X21", "L20", "D10", "P11", "D13",
+            "P33", "D12", "P32", "D11", "X31", "P30", "P22", "X11", "P20", "P10", "P23", "P21",
+            "X30", "X10", "M31", "X20", "M33", "M32", "M11", "M01", "M30", "M13", "M20", "M12",
+            "M21", "M10", "M23", "M22", "F00", "F02", "M03", "F03", "F01",
         ),
         (
-            "P02", "R00", "T10", "P03", "P00", "P01", "T20", "X00", "T30", "L12", "L10", "S00",
-            "L11", "D02", "P12", "L13", "D00", "D03", "L30", "P10", "P11", "L31", "P13", "X20",
-            "D01", "L32", "L33", "P31", "P32", "L20", "P30", "L22", "P33", "L21", "X30", "D10",
-            "P20", "X10", "L23", "P22", "D12", "P23", "D11", "D13", "P21", "X01", "X31", "X11",
-            "X21", "M30", "M32", "M33", "M03", "M10", "M31", "M00", "M12", "M13", "M20", "M21",
-            "M11", "M02", "M22", "M23", "F00", "F02", "F03", "M01", "F01",
+            "D12", "D10", "D13", "D00", "T10", "D02", "D01", "T20", "D03", "S00", "D11", "P02",
+            "P03", "L20", "P00", "P01", "P20", "L22", "L21", "L13", "R00", "P21", "T30", "P13",
+            "L10", "L23", "P22", "L11", "P10", "P23", "L12", "L33", "P33", "P11", "X00", "L30",
+            "P30", "L31", "P12", "P31", "X21", "L32", "P32", "X01", "X11", "M01", "M02", "X31",
+            "M20", "M03", "M22", "M23", "M21", "M30", "M31", "X30", "M32", "M00", "F03", "F02",
+            "M10", "F01", "M33", "M11", "X10", "M12", "X20", "M13", "F00",
         ),
     ),
 }

time: 71.2 us -> 70.1 us (0.985)
  the two profiles are of different devices: /device:TPU:1 before, /device:TPU:0 now
where the time goes in v4:
time: 70.1 us; the launch traced here: 70 us
  Pallas kernels  69.1 us (99%)
  local copies, waits for them, and re-layouts  0.8 us (1%)
    pallas_call x1, Pallas kernels, fused(): pl.pallas_call(functools.partial(fused_kernel, n_sp, n_tp, capacity), out...  69.1 us

profile of v4, /device:TPU:0, one launch (start us, length us, event | category | flops | bytes accessed | tf_op | source)
XLA Modules:
  0.0 70.0 jit_solution(14830134525857521391)
XLA Ops:
  0.0 69.1 %shard_map.163 = bf16[128,2048]{1,0:T(8,128)(2,1)S(1)} custom-call(bf16[256,512]{1,0:T(8,128)(2,1)} %refs_0_.1, bf16[256,512]{1,0:T(8,128)(2,1)} %refs_1_.1, bf16[31,512]{1,0:T(8,128)(2,1)} %refs_2_.1, s32[1,256]{1,0:T(1,128)} %bitcast.9, f32[1,512]{1,0:T(1,128)} %bitcast.7, f32[1,512]{1,0:T(1,128)} %bitcast.8, bf16[128,2048]{1,0:T(8,128)(2,1)} %refs_6_.1, ...), custom_call_target="tpu_custom_call" | custom-call | tf_op jit(solution)/shard_map/pallas_call | solution.py:731
  69.2 0.8 %copy.19 = bf16[128,2048]{1,0:T(8,128)(2,1)} copy(bf16[128,2048]{1,0:T(8,128)(2,1)S(1)} %shard_map.163) | data formatting | bytes 1048576

commit v5 on v4

--- a/solution.py
+++ b/solution.py
@@ -146,36 +146,36 @@
 ORDERS = {
     "E": (
         (
-            "D00", "T20", "P03", "P02", "P00", "X01", "D02", "D03", "D01", "P01", "X11", "T30",
-            "X21", "S00", "P32", "P22", "P31", "T10", "P30", "P33", "X31", "P21", "P20", "P23",
-            "X30", "P12", "P10", "P11", "M31", "M33", "M32", "P13", "X20", "X00", "M30", "M20",
-            "M21", "X10", "M23", "M22", "M01", "M02", "M10", "F01", "M03", "M00", "M13", "F03",
-            "M12", "M11", "F02", "F00",
+            "P00", "D01", "P02", "D03", "D00", "T10", "P03", "P01", "D02", "S00", "P11", "T20",
+            "P10", "P13", "P12", "P21", "T30", "P20", "X01", "X10", "P22", "P23", "X00", "P30",
+            "P33", "P31", "M10", "P32", "M12", "M11", "X20", "M13", "M03", "X30", "M20", "M02",
+            "M22", "M01", "M23", "M30", "M31", "M32", "X31", "M33", "M21", "M00", "X21", "X11",
+            "F02", "F01", "F00", "F03",
         ),
         (
-            "P02", "P03", "P00", "D03", "D01", "D00", "P01", "T20", "T10", "D02", "P10", "P13",
-            "P12", "P11", "P22", "P20", "T30", "P21", "P23", "X01", "P33", "X21", "X11", "M02",
-            "P30", "M01", "M03", "M20", "P32", "P31", "M22", "M21", "M12", "M11", "M23", "M13",
-            "X31", "M30", "M31", "X30", "M32", "S00", "M33", "X00", "X20", "M10", "X10", "M00",
-            "F00", "F01", "F02", "F03",
+            "S00", "T10", "D02", "P02", "P00", "T30", "P01", "P03", "X00", "D00", "D03", "D01",
+            "X01", "X10", "X20", "T20", "P30", "P32", "M00", "X30", "P31", "P33", "P23", "P21",
+            "P11", "P22", "P20", "X31", "P10", "P12", "P13", "M30", "M31", "X21", "M33", "M32",
+            "M03", "M20", "M23", "M22", "M21", "X11", "M10", "M13", "M01", "M12", "M11", "M02",
+            "F00", "F03", "F01", "F02",
         ),
     ),
     "I": (
         (
-            "P02", "P03", "P01", "T10", "L10", "P00", "R00", "T20", "L12", "T30", "P12", "D02",
-            "X00", "L11", "L30", "S00", "L13", "L22", "L32", "D03", "L31", "D01", "L33", "P13",
-            "D00", "X01", "P31", "M02", "L21", "L23", "M00", "X21", "L20", "D10", "P11", "D13",
-            "P33", "D12", "P32", "D11", "X31", "P30", "P22", "X11", "P20", "P10", "P23", "P21",
-            "X30", "X10", "M31", "X20", "M33", "M32", "M11", "M01", "M30", "M13", "M20", "M12",
-            "M21", "M10", "M23", "M22", "F00", "F02", "M03", "F03", "F01",
+            "P03", "D00", "D10", "D11", "D01", "D02", "D13", "P01", "D03", "D12", "T10", "P00",
+            "T20", "L21", "L20", "L11", "P11", "P20", "L22", "L13", "P02", "R00", "X01", "L10",
+            "P21", "L12", "L23", "P22", "P10", "T30", "L31", "L33", "P31", "P23", "P13", "P33",
+            "L30", "S00", "P12", "P30", "L32", "P32", "X00", "X10", "X20", "X30", "M00", "M20",
+            "M22", "M23", "M01", "M30", "M31", "X31", "M32", "M03", "M02", "M33", "M10", "F03",
+            "F00", "M11", "M21", "X11", "M12", "M13", "X21", "F02", "F01",
         ),
         (
-            "D12", "D10", "D13", "D00", "T10", "D02", "D01", "T20", "D03", "S00", "D11", "P02",
-            "P03", "L20", "P00", "P01", "P20", "L22", "L21", "L13", "R00", "P21", "T30", "P13",
-            "L10", "L23", "P22", "L11", "P10", "P23", "L12", "L33", "P33", "P11", "X00", "L30",
-            "P30", "L31", "P12", "P31", "X21", "L32", "P32", "X01", "X11", "M01", "M02", "X31",
-            "M20", "M03", "M22", "M23", "M21", "M30", "M31", "X30", "M32", "M00", "F03", "F02",
-            "M10", "F01", "M33", "M11", "X10", "M12", "X20", "M13", "F00",
+            "P01", "P03", "T10", "T20", "P02", "P00", "R00", "X01", "L10", "L13", "L12", "M02",
+            "T30", "X00", "M03", "L30", "D01", "D11", "L11", "P30", "L33", "D03", "D02", "P13",
+            "L32", "P33", "P32", "P11", "D10", "P12", "L21", "L31", "X20", "L22", "D00", "L23",
+            "P31", "D12", "P10", "X30", "S00", "L20", "P20", "D13", "P22", "P23", "M01", "X31",
+            "P21", "X10", "X11", "X21", "M31", "M30", "M33", "M11", "M32", "M10", "M20", "M13",
+            "M23", "M00", "M22", "M12", "M21", "F00", "F02", "F03", "F01",
         ),
     ),
 }
@@ -361,6 +361,7 @@
     )
     lot = tokens // CHUNK
     late = lot + 2
+    greeted = 2 * (1 - (plane + PLANES - 1) // PLANES)
 
     first = plane * per
     tri_r = lax.broadcasted_iota(jnp.int32, (tokens, tokens), 0)
@@ -397,7 +398,7 @@
         lows[b] = (mix - high.astype(F32)).astype(BF16)
 
     def conv_step(i, carry):
-        @pl.when(i == 0)
+        @pl.when(i == greeted)
         def _():
             pl.semaphore_wait(barrier, per - 1 + 1 + inner_count + has_next + has_last)
 

time: 70.1 us -> 72.2 us (1.030)
  the two profiles are of different devices: /device:TPU:0 before, /device:TPU:1 now
where the time goes in v5:
time: 72.2 us; the launch traced here: 71.5 us
  Pallas kernels  70.7 us (98%)
  local copies, waits for them, and re-layouts  0.8 us (1%)
    pallas_call x1, Pallas kernels, fused(): pl.pallas_call(functools.partial(fused_kernel, n_sp, n_tp, capacity), out...  70.7 us

profile of v5, /device:TPU:1, one launch (start us, length us, event | category | flops | bytes accessed | tf_op | source)
XLA Modules:
  0.0 71.5 jit_solution(8882410411419617124)
XLA Ops:
  0.0 70.7 %shard_map.163 = bf16[128,2048]{1,0:T(8,128)(2,1)S(1)} custom-call(bf16[256,512]{1,0:T(8,128)(2,1)} %refs_0_.1, bf16[256,512]{1,0:T(8,128)(2,1)} %refs_1_.1, bf16[31,512]{1,0:T(8,128)(2,1)} %refs_2_.1, s32[1,256]{1,0:T(1,128)} %bitcast.9, f32[1,512]{1,0:T(1,128)} %bitcast.7, f32[1,512]{1,0:T(1,128)} %bitcast.8, bf16[128,2048]{1,0:T(8,128)(2,1)} %refs_6_.1, ...), custom_call_target="tpu_custom_call" | custom-call | tf_op jit(solution)/shard_map/pallas_call | solution.py:732
  70.7 0.8 %copy.19 = bf16[128,2048]{1,0:T(8,128)(2,1)} copy(bf16[128,2048]{1,0:T(8,128)(2,1)S(1)} %shard_map.163) | data formatting | bytes 1048576
